TPU v7x, 32 devices: a whole 2x2x4 slice. The times are simulated.
32 devices in a mesh: dp: 4 (over y, x), kv: 4 (over z), tp: 2 (over core).
Axes of the slice: x: 2, y: 2, z: 4, core: 2. Of those that a mesh axis runs over, the one named last changes fastest.
Arguments:
- tokens: bfloat16 [8192, 2048], P(('dp', 'kv')), parts along dimension 0, may hold values from -60 to 60, as said below
- chosen: int32 [128, 16], P(('dp', 'kv')), parts along dimension 0, may hold values from -1 to 31, as said below
- query_weight: bfloat16 [2048, 1024], P('kv', 'tp'), may hold values from -0.125 to 0.125
- key_matrix: bfloat16 [2048, 128], P('kv', 'tp'), may hold values from -0.125 to 0.125
- value_matrix: bfloat16 [2048, 128], P('kv', 'tp'), may hold values from -0.125 to 0.125
- out_weight: bfloat16 [1024, 2048], P('tp', 'kv'), may hold values from -0.1875 to 0.1875
- out_gain: float32 [2048], replicated, may hold values from 0.1 to 1.9
Outputs:
- mixed_out: bfloat16 [8192, 2048], P(('dp', 'kv', 'tp')), parts along dimension 0
There are 4 independent parts, one for each index of `dp`. A program takes and returns all parts, laid end to end along the dimension named above; an argument that names none is the same for every part. Nothing has to cross between parts.
Inputs may be any that keep to these rules, and one draw needn't show every extreme that they name: tokens are of order one apart from few rows. chosen[g, 0] = g; every other entry of row g is -1 or a block below g, and the entries of a row other than -1 are distinct; the blocks that the rows of one device name on any single other device are at most 2 different ones, and this is reached.
All inputs are finite; a program needn't handle non-finite values.
Results may differ from a plain program's by a relative error of at most 0.012.
The roundings to bfloat16 on the way count: a program that leaves them out, or rounds other values in their place, can miss the bound.
Values may be sent and summed in bfloat16 or wider, within the bound.
No kernel may reach another device: no remote copies, remote signals or barrier semaphores. Data moves between devices by JAX's collectives and lax.ppermute only.
A program may use at most 64 MiB of HBM per device.

v0:
```python
import jax
import jax.numpy as jnp
from jax import lax
from jax.sharding import PartitionSpec as P

HEAD_WIDTH = 64
BLOCK_LENGTH = 64


def per_device(tokens, chosen, query_weight, key_matrix, value_matrix, out_weight, out_gain):
    tok_rows = tokens.shape[0]
    blocks = tok_rows // BLOCK_LENGTH
    device = lax.axis_index("kv")
    kv_count = lax.axis_size("kv")
    whole_query, whole_key, whole_value = (
        lax.all_gather(query_weight, "kv", axis=0, tiled=True),
        lax.all_gather(key_matrix, "kv", axis=0, tiled=True),
        lax.all_gather(value_matrix, "kv", axis=0, tiled=True),
    )
    query_rows = jnp.dot(tokens, whole_query, preferred_element_type=jnp.float32).astype(
        jnp.bfloat16
    )
    key_rows = jnp.dot(tokens, whole_key, preferred_element_type=jnp.float32).astype(jnp.bfloat16)
    value_rows = jnp.dot(tokens, whole_value, preferred_element_type=jnp.float32).astype(
        jnp.bfloat16
    )
    paired = jnp.concatenate([key_rows, value_rows], axis=1)
    pair_width = paired.shape[1]
    safe_ids = jnp.maximum(chosen, 0)
    everyone = lax.all_gather(paired, "kv", axis=0, tiled=True).reshape(
        kv_count * blocks, BLOCK_LENGTH, pair_width
    )
    picked = jnp.take(everyone, safe_ids, axis=0)
    head_count = query_rows.shape[1] // HEAD_WIDTH
    grouped = query_rows.reshape(blocks, BLOCK_LENGTH, head_count, HEAD_WIDTH)
    offsets = jnp.arange(BLOCK_LENGTH, dtype=jnp.int32)
    query_pos = (device * blocks + jnp.arange(blocks, dtype=jnp.int32))[
        :, None
    ] * BLOCK_LENGTH + offsets[None, :]
    key_pos = safe_ids[:, :, None] * BLOCK_LENGTH + offsets[None, None, :]
    visible = (chosen >= 0)[:, None, :, None] & (
        key_pos[:, None, :, :] <= query_pos[:, :, None, None]
    )

    def attend_block(inputs):
        query_block, pair_block, seen = inputs
        block_keys = pair_block[..., :HEAD_WIDTH]
        block_values = pair_block[..., HEAD_WIDTH:]
        scores = jnp.einsum(
            "qgd,skd->gqsk", query_block, block_keys, preferred_element_type=jnp.float32
        ) * HEAD_WIDTH ** (-0.5)
        scores = jnp.where(seen[None], scores, -1e30)
        row_max = jnp.max(scores, axis=(2, 3), keepdims=True)
        expon = jnp.exp(scores - row_max)
        row_sum = jnp.sum(expon, axis=(2, 3), keepdims=True)
        weights_bf = (expon / row_sum).astype(jnp.bfloat16)
        result = jnp.einsum(
            "gqsk,skd->qgd", weights_bf, block_values, preferred_element_type=jnp.float32
        )
        return result.astype(jnp.bfloat16)

    attended = lax.map(attend_block, (grouped, picked, visible))
    attended = attended.reshape(tok_rows, head_count * HEAD_WIDTH)
    whole_out = lax.all_gather(out_weight, "kv", axis=1, tiled=True)
    mixed = lax.psum_scatter(
        jnp.dot(attended, whole_out, preferred_element_type=jnp.float32).astype(jnp.bfloat16),
        "tp",
        scatter_dimension=0,
        tiled=True,
    ).astype(jnp.float32)
    normed = mixed * lax.rsqrt(jnp.mean(mixed * mixed, axis=-1, keepdims=True) + 1e-06) * out_gain
    return normed.astype(jnp.bfloat16)


def solution(mesh):
    placed = (
        P(("dp", "kv"), None),
        P(("dp", "kv"), None),
        P("kv", "tp"),
        P("kv", "tp"),
        P("kv", "tp"),
        P("tp", "kv"),
        P(),
    )
    return jax.shard_map(
        per_device,
        mesh=mesh,
        in_specs=placed,
        out_specs=P(("dp", "kv", "tp"), None),
        check_vma=False,
    )
```

profile of v0, /device:TPU:0, one launch (start us, length us, event | category | flops | bytes accessed | tf_op | source)
XLA Modules:
  0.0 154.0 jit_solution(18030068477290165004)
XLA Ops:
  6.5 0.7 all-gather.3.cloned.1.call-update
  7.3 0.7 all-gather.5.cloned.1.call-update
  8.1 0.7 broadcast_multiply_fusion
  8.7 0.7 broadcast_compare_fusion.1
  9.5 16.8 %all_gather.16 = bf16[2048,64]{0,1:T(8,128)(2,1)S(1)} all-gather(bf16[512,64]{0,1:T(8,128)(2,1)} %param.13), channel_id=1, replica_groups=mesh['dp'=4,'kv'=4,'tp'=2] {'kv'}, dimensions={0}, use_global_device_ids=true | all-gather | bytes 327680 | tf_op jit(solution)/shard_map/all_gather | solution.py:18
  26.4 17.1 %all_gather.15 = bf16[2048,64]{0,1:T(8,128)(2,1)S(1)} all-gather(bf16[512,64]{0,1:T(8,128)(2,1)} %param.12), channel_id=1, replica_groups=mesh['dp'=4,'kv'=4,'tp'=2] {'kv'}, dimensions={0}, use_global_device_ids=true | all-gather | bytes 327680 | tf_op jit(solution)/shard_map/all_gather | solution.py:17
  43.5 0.8 convolution_convert_fusion.2
  44.3 0.8 convolution_convert_fusion.3
  45.1 22.0 %all_gather.17 = bf16[2048,128]{0,1:T(8,128)(2,1)S(1)} all-gather(bf16[512,128]{0,1:T(8,128)(2,1)S(1)} %pad_maximum_fusion), channel_id=1, replica_groups=mesh['dp'=4,'kv'=4,'tp'=2] {'kv'}, dimensions={0}, use_global_device_ids=true | all-gather | bytes 655360 | tf_op jit(solution)/shard_map/all_gather | solution.py:30
  67.6 2.2 %gather_fusion = bf16[128,64,128]{2,1,0:T(8,128)(2,1)} fusion(bf16[32,64,128]{2,1,0:T(8,128)(2,1)S(1)} %bitcast.82, s32[1024]{0:T(1024)S(1)} %pad_clamp_fusion), kind=kCustom, calls=%fused_computation | custom fusion | bytes 4194816 | tf_op jit(solution)/shard_map/jit(_take)/gather | solution.py:33
  69.7 3.2 %broadcast_select_fusion = bf16[8,16,64,128]{3,2,1,0:T(8,128)(2,1)} fusion(bf16[8,16,64,128]{3,2,1,0:T(8,128)(2,1)} %bitcast.83, pred[8,16]{1,0:T(8,128)(4,1)S(1)} %get-tuple-element.56), kind=kLoop, calls=%fused_computation.27 | loop fusion | flops 1048576 | bytes 4194432 | tf_op jit(solution)/shard_map/jit(_take)/select_n | solution.py:33
  72.9 1.5 compare_and_fusion
  74.5 3.6 %convolution_convert_fusion.1 = bf16[512,512]{1,0:T(8,128)(2,1)} fusion(bf16[512,2048]{1,0:T(8,128)(2,1)S(1)} %copy-done, bf16[2048,512]{1,0:T(8,128)(2,1)} %all-gather.3.cloned.1.call-done), kind=kOutput, calls=%fused_computation.28 | convolution fusion | flops 1074003968 | bytes 4718592 | tf_op jit(solution)/shard_map/dot_general | solution.py:20
  78.1 2.4 %reshape.58 = bf16[8,64,8,64]{3,2,1,0:T(8,128)(2,1)} reshape(bf16[512,512]{1,0:T(8,128)(2,1)} %convolution_convert_fusion.1) | data formatting | bytes 1048576 | tf_op jit(solution)/shard_map/reshape | solution.py:35
  80.5 47.3 %while.10 = (s32[]{:T(128)}, bf16[8,64,8,64]{3,2,1,0:T(8,128)(2,1)}, bf16[8,16,64,128]{3,2,1,0:T(8,128)(2,1)}, pred[8,64,16,64]{1,3,2,0:T(8,128)(4,1)S(1)}, bf16[8,64,8,64]{3,2,1,0:T(8,128)(2,1)}, /*index=5*/s32[]{:T(128)}) while((s32[]{:T(128)}, bf16[8,64,8,64]{3,2,1,0:T(8,128)(2,1)}, bf16[8,16,64,128]{3,2,1,0:T(8,128)(2,1)}, ...), condition=%wide.region_3.4_spmd, body=%wide.region_0.3_spmd.sunk | while | flops 140540928 | bytes 8268369 | solution.py:62
  80.5 1.0 dynamic-slice_bitcast_fusion.5
  81.5 0.9 constant_dynamic-slice_fusion.2
  82.4 0.9 fusion.23
  83.3 1.0 fusion.24
  84.3 1.2 fusion.25
  85.7 0.7 constant_dynamic-update-slice_fusion.2
  86.4 1.0 dynamic-slice_bitcast_fusion.5
  87.4 0.9 constant_dynamic-slice_fusion.2
  88.3 0.9 fusion.23
  89.2 1.0 fusion.24
  90.2 1.2 fusion.25
  91.6 0.7 constant_dynamic-update-slice_fusion.2
  92.3 1.0 dynamic-slice_bitcast_fusion.5
  93.3 0.9 constant_dynamic-slice_fusion.2
  94.2 0.9 fusion.23
  95.1 1.0 fusion.24
  96.2 1.2 fusion.25
  97.5 0.7 constant_dynamic-update-slice_fusion.2
  98.2 1.0 dynamic-slice_bitcast_fusion.5
  99.2 0.9 constant_dynamic-slice_fusion.2
  100.1 0.9 fusion.23
  101.0 1.0 fusion.24
  102.1 1.2 fusion.25
  103.5 0.7 constant_dynamic-update-slice_fusion.2
  104.1 1.0 dynamic-slice_bitcast_fusion.5
  105.1 0.9 constant_dynamic-slice_fusion.2
  106.0 0.9 fusion.23
  106.9 1.0 fusion.24
  108.0 1.2 fusion.25
  110.0 1.0 dynamic-slice_bitcast_fusion.5
  111.0 0.9 constant_dynamic-slice_fusion.2
  111.9 0.9 fusion.23
  112.9 1.0 fusion.24
  113.9 1.2 fusion.25
  116.0 1.0 dynamic-slice_bitcast_fusion.5
  116.9 0.9 constant_dynamic-slice_fusion.2
  117.9 0.9 fusion.23
  118.8 1.0 fusion.24
  119.8 1.2 fusion.25
  121.9 1.0 dynamic-slice_bitcast_fusion.5
  122.8 0.9 constant_dynamic-slice_fusion.2
  123.8 0.9 fusion.23
  124.7 1.0 fusion.24
  125.7 1.2 fusion.25
  127.8 1.9 %reshape.59 = bf16[512,512]{1,0:T(8,128)(2,1)S(1)} reshape(bf16[8,64,8,64]{3,2,1,0:T(8,128)(2,1)} %get-tuple-element.32) | data formatting | bytes 1048576 | tf_op jit(solution)/shard_map/reshape | solution.py:63
  129.7 4.2 %convolution_convert_fusion = bf16[512,2048]{1,0:T(8,128)(2,1)} fusion(bf16[512,512]{1,0:T(8,128)(2,1)S(1)} %reshape.59, bf16[512,2048]{1,0:T(8,128)(2,1)} %all-gather.5.cloned.1.call-done), kind=kOutput, calls=%fused_computation.21 | convolution fusion | flops 1074790400 | bytes 4718592 | tf_op jit(solution)/shard_map/dot_general | solution.py:66
  133.9 9.6 %reduce-scatter.2.cloned.1.call-done = bf16[256,2048]{1,0:T(8,128)(2,1)} async-done(((bf16[512,2048]{1,0:T(8,128)(2,1)}), bf16[256,2048]{1,0:T(8,128)(2,1)}) %reduce-scatter.2.cloned.1.call-update) | async-done | bytes 1048592 | tf_op jit(solution)/shard_map/reduce_scatter | solution.py:65
  143.5 1.5 fusion.9
  145.0 2.5 %fusion.11 = bf16[256,2048]{1,0:T(8,128)(2,1)} fusion(bf16[256,2048]{1,0:T(8,128)(2,1)} %reduce-scatter.2.cloned.1.call-done, f32[2048]{0:T(1024)S(1)} %copy-done.1, f32[256]{0:T(256)S(1)} %add_rsqrt_fusion), kind=kLoop, calls=%fused_computation.26 | loop fusion | flops 2097152 | bytes 2106368 | tf_op jit(solution)/shard_map/convert_element_type | solution.py:72
  (39 shorter events, 4.6 us)
Async XLA Ops:
  6.5 37.0 %copy-start = (bf16[512,2048]{1,0:T(8,128)(2,1)S(1)}, bf16[512,2048]{1,0:T(8,128)(2,1)}, u32[]{:S(2)}) copy-start(bf16[512,2048]{1,0:T(8,128)(2,1)} %param.9) | copy-start | bytes 6291460
  6.5 67.9 %all-gather.3.cloned.1.call-start = ((), (), s32[]{:S(2)}) async-start(), calls=%async_computation.1 | async-start | bytes 2621440 | tf_op jit(solution)/shard_map/all_gather | solution.py:16
  7.3 122.4 %all-gather.5.cloned.1.call-start = ((), (), s32[]{:S(2)}) async-start(), calls=%async_computation.2 | async-start | bytes 2621440 | tf_op jit(solution)/shard_map/all_gather | solution.py:64
  8.0 135.5 %reduce-scatter.2.cloned.1.call-start = ((), (), s32[]{:S(2)}) async-start(), calls=%async_computation.3 | async-start | bytes 3145728 | tf_op jit(solution)/shard_map/reduce_scatter | solution.py:65
  133.8 11.2 %copy-start.1 = (f32[2048]{0:T(1024)S(1)}, f32[2048]{0:T(1024)}, u32[]{:S(2)}) copy-start(f32[2048]{0:T(1024)} %param.15) | copy-start | bytes 24580
Sparse Core Ops, SparseCore 0:
  8.9 61.9 all-gather.2
  72.5 44.4 all-gather.4
  134.0 9.4 reduce-scatter.1
where the time goes:
time: 155 us; the launch traced here: 154 us
  blocking collectives  56 us (36%)
  local copies, waits for them, and re-layouts  28.5 us (18%)
  matrix products  26.5 us (17%)
  other arithmetic  18.5 us (12%)
  between operations  13.2 us (9%)
  waiting for transfers between devices  11.1 us (7%)
    all_gather x1, blocking collectives, per_device(): lax.all_gather(paired, 'kv', axis=0, tiled=True)  22 us
    all_gather x1, blocking collectives, per_device(): lax.all_gather(key_matrix, 'kv', axis=0, tiled=True)  17.1 us
    all_gather x1, blocking collectives, per_device(): lax.all_gather(value_matrix, 'kv', axis=0, tiled=True)  16.8 us
    dot_general x8, matrix products, attend_block(): jnp.einsum('gqsk,skd->qgd', weights_bf, block_values, preferred_element_t...  9.99 us
    reduce_scatter x1, waiting for transfers between devices, per_device(): lax.psum_scatter(jnp.dot(attended, whole_out, preferred_element_type=jnp....  9.61 us
    reduce_sum x8, other arithmetic, attend_block(): row_sum = jnp.sum(expon, axis=(2, 3), keepdims=True)  8.16 us
    squeeze x8, local copies, waits for them, and re-layouts, per_device(): attended = lax.map(attend_block, (grouped, picked, visible))  7.8 us
    dynamic_slice x8, local copies, waits for them, and re-layouts, per_device(): attended = lax.map(attend_block, (grouped, picked, visible))  7.37 us
  transfers between devices with their start and end apart: 3, of which 1 were waited for; matrix products, arithmetic and copies ran while one was open for 42% of the time, Pallas kernels for 0%

commit v1 on v0

v1 whole, which is shorter than its diff:
```python
import functools

import jax
import jax.numpy as jnp
from jax import lax
from jax.experimental import pallas as pl
from jax.experimental.pallas import tpu as pltpu
from jax.sharding import PartitionSpec as P

HEAD_WIDTH = 64
BLOCK_LENGTH = 64
ALIGN = 16
LOG2E = 1.4426950408889634
BF16 = jnp.bfloat16
F32 = jnp.float32


def shift(x, axis, by, count):
    return lax.ppermute(x, axis, [(i, (i + by) % count) for i in range(count)])


def swap(x, axis, bit, count):
    return lax.ppermute(x, axis, [(i, i ^ bit) for i in range(count)])


def spread(w, kv_count, dp_count):
    rows = w.shape[0] // dp_count
    half = rows // 2
    dp = lax.axis_index("dp")
    piece = lax.dynamic_slice_in_dim(w, dp * rows, rows, axis=0)
    got = [shift(piece, "kv", s, kv_count) for s in range(1, kv_count)]
    mine = jnp.concatenate([g[:half] for g in got] + [g[half:] for g in got], axis=0)
    cut = half * (kv_count - 1)
    across = swap(mine, "dp", 1, dp_count)
    along = swap(mine, "dp", 2, dp_count)
    far_top = swap(across[:cut], "dp", 2, dp_count)
    far_low = swap(along[cut:], "dp", 1, dp_count)
    return [w, mine, across, along, far_top, far_low]


def place(refs, dest, kv, dp, kv_count, dp_count):
    if len(refs) == 1:
        dest[...] = refs[0][...].reshape(dest.shape)
        return
    own, mine, across, along, far_top, far_low = refs
    dest[pl.ds(kv, 1)] = own[...][None]
    rows = own.shape[0] // dp_count
    half = rows // 2
    cut = half * (kv_count - 1)
    for s in range(1, kv_count):
        source = lax.rem(kv - s + kv_count, kv_count)
        at = half * (s - 1)
        for h in range(2):
            for bits, ref, base in (
                (0, mine, h * cut),
                (1, across, h * cut),
                (2, along, h * cut),
                (3, (far_top, far_low)[h], 0),
            ):
                first = pl.multiple_of((dp ^ bits) * rows + h * half, half)
                dest[pl.ds(source, 1), pl.ds(first, half)] = ref[pl.ds(base + at, half)][None]


def attend_kernel(where_ref, chosen_ref, tok_ref, *refs, n_weights, n_rows, kv_count, dp_count, heads):
    w_refs = refs[:n_weights]
    row_refs = refs[n_weights:n_weights + n_rows]
    out_ref, w_full, kv_full, q_full, picked = refs[n_weights + n_rows:]
    kv = where_ref[0]
    dp = where_ref[1]
    place(w_refs, w_full, kv, dp, kv_count, dp_count)
    if n_rows == 1:
        kv_full[...] = row_refs[0][...]
    else:
        count = row_refs[0].shape[0]
        for s, ref in enumerate(row_refs):
            source = lax.rem(kv - s + kv_count, kv_count)
            kv_full[pl.ds(pl.multiple_of(source * count, count), count)] = ref[...]
    whole = w_full[...].reshape(-1, w_full.shape[-1])
    queries = jnp.dot(tok_ref[...], whole, preferred_element_type=F32).astype(BF16)
    q_full[...] = queries
    blocks, sel = chosen_ref.shape
    wide = heads * BLOCK_LENGTH
    key_at = lax.broadcasted_iota(jnp.int32, (BLOCK_LENGTH, wide), 0)
    query_at = lax.rem(lax.broadcasted_iota(jnp.int32, (BLOCK_LENGTH, wide), 1), BLOCK_LENGTH)
    causal = key_at <= query_at
    factor = HEAD_WIDTH ** (-0.5) * LOG2E

    def one_block(g, carry):
        at = pl.multiple_of(g * BLOCK_LENGTH, BLOCK_LENGTH)
        qg = q_full[pl.ds(at, BLOCK_LENGTH)]
        stacked = jnp.concatenate(
            [qg[:, h * HEAD_WIDTH:(h + 1) * HEAD_WIDTH] for h in range(heads)], axis=0
        )
        stacked = jnp.concatenate([stacked, jnp.zeros_like(stacked)], axis=1)
        bias = []
        for s in range(sel):
            name = chosen_ref[g, s]
            first = pl.multiple_of(jnp.maximum(name, 0) * BLOCK_LENGTH, BLOCK_LENGTH)
            picked[s * BLOCK_LENGTH:(s + 1) * BLOCK_LENGTH] = kv_full[pl.ds(first, BLOCK_LENGTH)]
            bias.append(jnp.where(name < 0, F32(-1e30), F32(0)))
        pairs = picked[...]
        scores = lax.dot_general(
            pairs, stacked, (((1,), (1,)), ((), ())), preferred_element_type=F32
        )
        parts = []
        top = None
        for s in range(sel):
            part = scores[s * BLOCK_LENGTH:(s + 1) * BLOCK_LENGTH]
            part = jnp.where(causal, part, -1e30) if s == 0 else part + bias[s]
            parts.append(part)
            peak = jnp.max(part, axis=0, keepdims=True)
            top = peak if top is None else jnp.maximum(top, peak)
        total = None
        probs = []
        for part in parts:
            e = jnp.exp2((part - top) * factor)
            add = jnp.sum(e, axis=0, keepdims=True)
            total = add if total is None else total + add
            probs.append(e.astype(BF16))
        prob = jnp.concatenate(probs, axis=0)
        mixed = lax.dot_general(
            pairs, prob, (((0,), (0,)), ((), ())), preferred_element_type=F32
        )
        outcome = (mixed[HEAD_WIDTH:] / total).T
        out_ref[pl.ds(at, BLOCK_LENGTH)] = jnp.concatenate(
            [outcome[h * BLOCK_LENGTH:(h + 1) * BLOCK_LENGTH] for h in range(heads)], axis=1
        ).astype(BF16)
        return carry

    lax.fori_loop(0, blocks, one_block, 0)


def project_kernel(where_ref, att_ref, *refs, n_weights, kv_count, dp_count):
    w_refs = refs[:n_weights]
    mine_ref, other_ref, w_full = refs[n_weights:]
    tp = where_ref[2]
    half = mine_ref.shape[0]
    width = w_full.shape[2]
    place(w_refs, w_full, where_ref[0], where_ref[1], kv_count, dp_count)
    for out, which in ((other_ref, 1 - tp), (mine_ref, tp)):
        rows = att_ref[pl.ds(pl.multiple_of(which * half, half), half)]
        for k in range(w_full.shape[0]):
            out[:, k * width:(k + 1) * width] = jnp.dot(
                rows, w_full[k], preferred_element_type=F32
            ).astype(BF16)


def norm_kernel(a_ref, b_ref, gain_ref, out_ref):
    mixed = a_ref[...].astype(F32) + b_ref[...].astype(F32)
    scale = lax.rsqrt(jnp.mean(mixed * mixed, axis=-1, keepdims=True) + 1e-06)
    out_ref[...] = (mixed * scale * gain_ref[...]).astype(BF16)


def per_device(tokens, chosen, query_weight, key_matrix, value_matrix, out_weight, out_gain):
    kv_count = lax.axis_size("kv")
    dp_count = lax.axis_size("dp")
    tp_count = lax.axis_size("tp")
    kv = lax.axis_index("kv")
    dp = lax.axis_index("dp")
    tp = lax.axis_index("tp")
    where = jnp.stack([kv, dp, tp]).astype(jnp.int32)
    tok_rows, model = tokens.shape
    heads = query_weight.shape[1] // HEAD_WIDTH
    shard = query_weight.shape[0]
    direct = (
        dp_count == 4
        and kv_count <= 8
        and shard % (2 * dp_count * ALIGN) == 0
        and out_weight.shape[1] % 128 == 0
    )
    pair_shard = jnp.concatenate([key_matrix, value_matrix], axis=1)
    if direct:
        pair_parts = spread(pair_shard, kv_count, dp_count)
        q_parts = spread(query_weight, kv_count, dp_count)
        o_parts = spread(out_weight, kv_count, dp_count)
        pair_kernel = functools.partial(
            pair_project, n_weights=len(pair_parts), kv_count=kv_count, dp_count=dp_count
        )
    else:
        pair_parts = [lax.all_gather(pair_shard, "kv", axis=0, tiled=True)]
        q_parts = [lax.all_gather(query_weight, "kv", axis=0, tiled=True)]
        o_parts = [lax.all_gather(out_weight, "kv", axis=1, tiled=True)]
        pair_kernel = functools.partial(
            pair_project, n_weights=1, kv_count=kv_count, dp_count=dp_count
        )
    vmem = pl.BlockSpec(memory_space=pltpu.VMEM)
    smem = pl.BlockSpec(memory_space=pltpu.SMEM)
    pair_width = pair_shard.shape[1]
    pairs = pl.pallas_call(
        pair_kernel,
        out_shape=jax.ShapeDtypeStruct((tok_rows, pair_width), BF16),
        in_specs=[smem, vmem] + [vmem] * len(pair_parts),
        out_specs=vmem,
        scratch_shapes=[pltpu.VMEM((kv_count, shard, pair_width), BF16)]
        if direct
        else [pltpu.VMEM((1, model, pair_width), BF16)],
    )(where, tokens, *pair_parts)
    if direct:
        row_parts = [pairs] + [
            lax.ppermute(pairs, "kv", [(i, i + s) for i in range(kv_count - s)])
            for s in range(1, kv_count)
        ]
    else:
        row_parts = [lax.all_gather(pairs, "kv", axis=0, tiled=True)]
    attended = pl.pallas_call(
        functools.partial(
            attend_kernel,
            n_weights=len(q_parts),
            n_rows=len(row_parts),
            kv_count=kv_count,
            dp_count=dp_count,
            heads=heads,
        ),
        out_shape=jax.ShapeDtypeStruct((tok_rows, heads * HEAD_WIDTH), BF16),
        in_specs=[smem, smem, vmem] + [vmem] * (len(q_parts) + len(row_parts)),
        out_specs=vmem,
        scratch_shapes=[
            pltpu.VMEM((kv_count, shard, heads * HEAD_WIDTH) if direct else (1, model, heads * HEAD_WIDTH), BF16),
            pltpu.VMEM((kv_count * tok_rows, pair_width), BF16),
            pltpu.VMEM((tok_rows, heads * HEAD_WIDTH), BF16),
            pltpu.VMEM((chosen.shape[1] * BLOCK_LENGTH, pair_width), BF16),
        ],
    )(where, chosen, tokens, *q_parts, *row_parts)
    out_rows = tok_rows // tp_count
    head_rows, out_cols = out_weight.shape
    columns = out_cols * kv_count
    piece = jax.ShapeDtypeStruct((out_rows, columns), BF16)
    mine, other = pl.pallas_call(
        functools.partial(
            project_kernel, n_weights=len(o_parts), kv_count=kv_count, dp_count=dp_count
        ),
        out_shape=(piece, piece),
        in_specs=[smem, vmem] + [vmem] * len(o_parts),
        out_specs=(vmem, vmem),
        scratch_shapes=[
            pltpu.VMEM((kv_count, head_rows, out_cols) if direct else (1, head_rows, columns), BF16)
        ],
    )(where, attended, *o_parts)
    theirs = swap(other, "tp", 1, tp_count)
    return pl.pallas_call(
        norm_kernel,
        out_shape=jax.ShapeDtypeStruct((out_rows, columns), BF16),
        in_specs=[vmem, vmem, vmem],
        out_specs=vmem,
    )(mine, theirs, out_gain.reshape(1, -1))


def pair_project(where_ref, tok_ref, *refs, n_weights, kv_count, dp_count):
    w_refs = refs[:n_weights]
    out_ref, w_full = refs[n_weights:]
    place(w_refs, w_full, where_ref[0], where_ref[1], kv_count, dp_count)
    whole = w_full[...].reshape(-1, w_full.shape[-1])
    out_ref[...] = jnp.dot(tok_ref[...], whole, preferred_element_type=F32).astype(BF16)


def solution(mesh):
    placed = (
        P(("dp", "kv"), None),
        P(("dp", "kv"), None),
        P("kv", "tp"),
        P("kv", "tp"),
        P("kv", "tp"),
        P("tp", "kv"),
        P(),
    )
    return jax.shard_map(
        per_device,
        mesh=mesh,
        in_specs=placed,
        out_specs=P(("dp", "kv", "tp"), None),
        check_vma=False,
    )
```

time: 155 us -> 111 us (0.72)
  blocking collectives: 56 us -> 0 us
  starting transfers between devices: 0.08 us -> 37.6 us
  matrix products: 26.5 us -> 0 us
  waiting for transfers between devices: 11.1 us -> 37.5 us
  Pallas kernels: 0 us -> 25 us
  local copies, waits for them, and re-layouts: 28.5 us -> 8.22 us
  other arithmetic: 18.5 us -> 1.49 us
  between operations: 13.2 us -> 0.42 us
    all_gather x3 -> x0, blocking collectives: 56 us -> none  [the longest x1 22 us: per_device(): lax.all_gather(paired, 'kv', axis=0, tiled=True)]
    ppermute x0 -> x25, starting transfers between devices: none -> 37.6 us  [the longest x9 18.4 us: shift(): return lax.ppermute(x, axis, [(i, (i + by) % count) for i in range(count)])]
    ppermute x0 -> x25, waiting for transfers between devices: none -> 37.5 us  [the longest x13 20.2 us: swap(): return lax.ppermute(x, axis, [(i, i ^ bit) for i in range(count)])]
    dot_general x20 -> x0, matrix products: 26.5 us -> none  [the longest x8 9.99 us: attend_block(): jnp.einsum('gqsk,skd->qgd', weights_bf, block_values, preferred_element_t...]
    pallas_call x0 -> x4, Pallas kernels: none -> 25 us  [the longest x1 14.5 us: per_device(): pl.pallas_call(functools.partial(attend_kernel, n_weights=len(q_parts), n...]
    reduce_sum x9 -> x0, other arithmetic: 9.67 us -> none  [the longest x8 8.16 us: attend_block(): row_sum = jnp.sum(expon, axis=(2, 3), keepdims=True)]
    reduce_scatter x1 -> x0, waiting for transfers between devices: 9.61 us -> none  [per_device(): lax.psum_scatter(jnp.dot(attended, whole_out, preferred_element_type=jnp....]
    squeeze x8 -> x0, local copies, waits for them, and re-layouts: 7.8 us -> none  [per_device(): attended = lax.map(attend_block, (grouped, picked, visible))]
  transfers between devices with their start and end apart: 3 -> 25, of which waited for: 1 -> 6; matrix products, arithmetic and copies ran while one was open for 42% -> 3% of each run, Pallas kernels for 0% -> 16%
where the time goes in v1:
time: 111 us; the launch traced here: 110 us
  starting transfers between devices  37.6 us (34%)
  waiting for transfers between devices  37.5 us (34%)
  Pallas kernels  25 us (23%)
  local copies, waits for them, and re-layouts  8.22 us (7%)
  other arithmetic  1.49 us (1%)
    ppermute x13, waiting for transfers between devices, swap(): return lax.ppermute(x, axis, [(i, i ^ bit) for i in range(count)])  20.2 us
    ppermute x9, starting transfers between devices, shift(): return lax.ppermute(x, axis, [(i, (i + by) % count) for i in range(count)])  18.4 us
    pallas_call x1, Pallas kernels, per_device(): pl.pallas_call(functools.partial(attend_kernel, n_weights=len(q_parts), n...  14.5 us
    ppermute x9, waiting for transfers between devices, shift(): return lax.ppermute(x, axis, [(i, (i + by) % count) for i in range(count)])  14.5 us
    ppermute x13, starting transfers between devices, swap(): return lax.ppermute(x, axis, [(i, i ^ bit) for i in range(count)])  13.6 us
    unnamed x55, local copies, waits for them, and re-layouts  6.31 us
    ppermute x3, starting transfers between devices, per_device(): lax.ppermute(pairs, 'kv', [(i, i + s) for i in range(kv_count - s)])  5.64 us
    pallas_call x1, Pallas kernels, per_device(): pl.pallas_call(functools.partial(project_kernel, n_weights=len(o_parts),...  4.05 us
  transfers between devices with their start and end apart: 25, of which 6 were waited for; matrix products, arithmetic and copies ran while one was open for 3% of the time, Pallas kernels for 16%

profile of v1, /device:TPU:0, one launch (start us, length us, event | category | flops | bytes accessed | tf_op | source)
XLA Modules:
  0.0 110.2 jit_solution(16550313078113615413)
XLA Ops:
  0.0 1.0 copy.8
  1.0 1.0 copy.9
  1.9 0.1 fusion
  2.0 5.1 %collective-permute-start.9 = (bf16[128,128]{1,0:T(8,128)(2,1)S(1)}, bf16[128,128]{1,0:T(8,128)(2,1)S(1)}, u32[]{:S(2)}, u32[]{:S(2)}) collective-permute-start(bf16[128,128]{1,0:T(8,128)(2,1)S(1)} %fusion), channel_id=1, source_target_pairs={{0,6},{2,0},{4,2},{6,4},{1,7},{3,1},{5,3},{7,5},{8,14},{10,8},{12,... | collective-permute-start | bytes 98312 | tf_op jit(solution)/shard_map/ppermute | solution.py:19
  7.2 0.0 collective-permute-start.8
  7.2 1.0 collective-permute-start.7
  8.2 0.9 constant_dynamic-slice_fusion
  9.1 2.9 %collective-permute-start.19 = (bf16[128,512]{1,0:T(8,128)(2,1)S(1)}, bf16[128,512]{1,0:T(8,128)(2,1)S(1)}, u32[]{:S(2)}, u32[]{:S(2)}) collective-permute-start(bf16[128,512]{1,0:T(8,128)(2,1)S(1)} %constant_dynamic-slice_fusion), channel_id=1, source_target_pairs={{0,6},{2,0},{4,2},{6,4},{1,7},{3,1},{5,3},{7,5},{8,14},{10,8},{12,... | collective-permute-start | bytes 393224 | tf_op jit(solution)/shard_map/ppermute | solution.py:19
  12.0 1.1 %collective-permute-start.18 = (bf16[128,512]{1,0:T(8,128)(2,1)S(1)}, bf16[128,512]{1,0:T(8,128)(2,1)S(1)}, u32[]{:S(2)}, u32[]{:S(2)}) collective-permute-start(bf16[128,512]{1,0:T(8,128)(2,1)S(1)} %constant_dynamic-slice_fusion), channel_id=1, source_target_pairs={{0,4},{2,6},{4,0},{6,2},{1,5},{3,7},{5,1},{7,3},{8,12},{10,14},{12... | collective-permute-start | bytes 393224 | tf_op jit(solution)/shard_map/ppermute | solution.py:19
  13.1 0.9 constant_dynamic-slice_fusion.1
  14.0 0.0 collective-permute-done.7
  14.0 0.1 collective-permute-start.17
  14.1 0.0 collective-permute-done.8
  14.1 3.8 %collective-permute-start.2 = (bf16[128,512]{1,0:T(8,128)(2,1)S(1)}, bf16[128,512]{1,0:T(8,128)(2,1)S(1)}, u32[]{:S(2)}, u32[]{:S(2)}) collective-permute-start(bf16[128,512]{1,0:T(8,128)(2,1)S(1)} %constant_dynamic-slice_fusion.1), channel_id=1, source_target_pairs={{0,6},{2,0},{4,2},{6,4},{1,7},{3,1},{5,3},{7,5},{8,14},{10,8},{12,... | collective-permute-start | bytes 393224 | tf_op jit(solution)/shard_map/ppermute | solution.py:19
  17.9 0.0 collective-permute-done.9
  17.9 0.0 collective-permute-start
  18.0 8.8 %collective-permute-done = bf16[128,512]{1,0:T(8,128)(2,1)S(1)} collective-permute-done((bf16[128,512]{1,0:T(8,128)(2,1)S(1)}, bf16[128,512]{1,0:T(8,128)(2,1)S(1)}, u32[]{:S(2)}, u32[]{:S(2)}) %collective-permute-start) | collective-permute-done | bytes 131104 | tf_op jit(solution)/shard_map/ppermute | solution.py:19
  26.8 4.4 %collective-permute-start.1 = (bf16[128,512]{1,0:T(8,128)(2,1)S(1)}, bf16[128,512]{1,0:T(8,128)(2,1)S(1)}, u32[]{:S(2)}, u32[]{:S(2)}) collective-permute-start(bf16[128,512]{1,0:T(8,128)(2,1)S(1)} %constant_dynamic-slice_fusion.1), channel_id=1, source_target_pairs={{0,4},{2,6},{4,0},{6,2},{1,5},{3,7},{5,1},{7,3},{8,12},{10,14},{12... | collective-permute-start | bytes 393224 | tf_op jit(solution)/shard_map/ppermute | solution.py:19
  31.2 5.7 %collective-permute-done.1 = bf16[128,512]{1,0:T(8,128)(2,1)S(1)} collective-permute-done((bf16[128,512]{1,0:T(8,128)(2,1)S(1)}, bf16[128,512]{1,0:T(8,128)(2,1)S(1)}, u32[]{:S(2)}, u32[]{:S(2)}) %collective-permute-start.1) | collective-permute-done | bytes 131104 | tf_op jit(solution)/shard_map/ppermute | solution.py:19
  36.8 1.5 %collective-permute-start.11 = (bf16[384,128]{1,0:T(8,128)(2,1)S(1)}, bf16[384,128]{1,0:T(8,128)(2,1)S(1)}, u32[]{:S(2)}, u32[]{:S(2)}) collective-permute-start(bf16[384,128]{1,0:T(8,128)(2,1)S(1)} %constant_dynamic-update-slice_fusion.refs_1_), channel_id=1, source_target_pairs={{0,16},{8,24},{16,0},{24,8},{1,17},{9,25},{17,1},{25,9},{2,18},{10... | collective-permute-start | bytes 294920 | tf_op jit(solution)/shard_map/ppermute | solution.py:23
  38.4 0.0 collective-permute-done.2
  38.4 1.6 %collective-permute-start.10 = (bf16[384,128]{1,0:T(8,128)(2,1)S(1)}, bf16[384,128]{1,0:T(8,128)(2,1)S(1)}, u32[]{:S(2)}, u32[]{:S(2)}) collective-permute-start(bf16[384,128]{1,0:T(8,128)(2,1)S(1)} %constant_dynamic-update-slice_fusion.refs_1_), channel_id=1, source_target_pairs={{0,8},{8,0},{16,24},{24,16},{1,9},{9,1},{17,25},{25,17},{2,10},{10... | collective-permute-start | bytes 294920 | tf_op jit(solution)/shard_map/ppermute | solution.py:23
  40.0 0.0 copy-start.5
  40.0 0.0 collective-permute-done.17
  40.0 0.6 collective-permute-start.4
  40.6 0.0 collective-permute-done.18
  40.6 0.6 collective-permute-start.3
  41.2 0.0 collective-permute-done.19
  41.2 1.6 %collective-permute-start.21 = (bf16[384,512]{1,0:T(8,128)(2,1)S(1)}, bf16[384,512]{1,0:T(8,128)(2,1)S(1)}, u32[]{:S(2)}, u32[]{:S(2)}) collective-permute-start(bf16[384,512]{1,0:T(8,128)(2,1)S(1)} %slice_dynamic-update-slice_fusion.refs_1_), channel_id=1, source_target_pairs={{0,16},{8,24},{16,0},{24,8},{1,17},{9,25},{17,1},{25,9},{2,18},{10... | collective-permute-start | bytes 1179656 | tf_op jit(solution)/shard_map/ppermute | solution.py:23
  42.8 0.0 collective-permute-done.11.refs_3_
  42.8 1.5 %collective-permute-start.20 = (bf16[384,512]{1,0:T(8,128)(2,1)S(1)}, bf16[384,512]{1,0:T(8,128)(2,1)S(1)}, u32[]{:S(2)}, u32[]{:S(2)}) collective-permute-start(bf16[384,512]{1,0:T(8,128)(2,1)S(1)} %slice_dynamic-update-slice_fusion.refs_1_), channel_id=1, source_target_pairs={{0,8},{8,0},{16,24},{24,16},{1,9},{9,1},{17,25},{25,17},{2,10},{10... | collective-permute-start | bytes 1179656 | tf_op jit(solution)/shard_map/ppermute | solution.py:23
  44.3 0.0 collective-permute-done.10.refs_2_
  44.3 1.2 %collective-permute-start.13 = (bf16[192,128]{1,0:T(8,128)(2,1)S(1)}, bf16[192,128]{1,0:T(8,128)(2,1)S(1)}, u32[]{:S(2)}, u32[]{:S(2)}) collective-permute-start(bf16[192,128]{1,0:T(8,128)(2,1)S(1)} %slice.111), channel_id=1, source_target_pairs={{0,8},{8,0},{16,24},{24,16},{1,9},{9,1},{17,25},{25,17},{2,10},{10... | collective-permute-start | bytes 147464 | tf_op jit(solution)/shard_map/ppermute | solution.py:23
  45.6 0.7 pad_maximum_fusion.refs_0_
  46.3 14.6 %collective-permute-done.13.refs_5_ = bf16[192,128]{1,0:T(8,128)(2,1)S(1)} collective-permute-done((bf16[192,128]{1,0:T(8,128)(2,1)S(1)}, bf16[192,128]{1,0:T(8,128)(2,1)S(1)}, u32[]{:S(2)}, u32[]{:S(2)}) %collective-permute-start.13) | collective-permute-done | bytes 49184 | tf_op jit(solution)/shard_map/ppermute | solution.py:23
  60.9 0.7 collective-permute-start.12
  61.7 0.7 pad_add_fusion.where_ref
  62.3 2.7 %collective-permute-done.12.refs_4_ = bf16[192,128]{1,0:T(8,128)(2,1)S(1)} collective-permute-done((bf16[192,128]{1,0:T(8,128)(2,1)S(1)}, bf16[192,128]{1,0:T(8,128)(2,1)S(1)}, u32[]{:S(2)}, u32[]{:S(2)}) %collective-permute-start.12) | collective-permute-done | bytes 49184 | tf_op jit(solution)/shard_map/ppermute | solution.py:23
  65.1 0.6 copy-done.18
  65.7 3.2 %shard_map.73.refs_6_ = bf16[512,128]{1,0:T(8,128)(2,1)} custom-call(s32[3]{0:T(128)} %pad_add_fusion.where_ref, bf16[512,2048]{1,0:T(8,128)(2,1)} %tok_ref.3, bf16[512,128]{1,0:T(8,128)(2,1)} %pad_maximum_fusion.refs_0_, bf16[384,128]{1,0:T(8,128)(2,1)} %copy-done.13, bf16[384,128]{1,0:T(8,128)(2,1)} %copy-done.8, bf16[384,128]{1,0:T(8,128)(2,1)} %copy-done.7, ...), custom_call_target="tpu_custom_call" | custom-call | tf_op jit(solution)/shard_map/pallas_call | solution.py:189
  68.8 1.3 %collective-permute-start.16 = (bf16[512,128]{1,0:T(8,128)(2,1)}, bf16[512,128]{1,0:T(8,128)(2,1)S(1)}, u32[]{:S(2)}, u32[]{:S(2)}) collective-permute-start(bf16[512,128]{1,0:T(8,128)(2,1)} %shard_map.73.refs_6_), channel_id=1, source_target_pairs={{0,6},{1,7},{8,14},{9,15},{16,22},{17,23},{24,30},{25,31}} | collective-permute-start | bytes 393224 | tf_op jit(solution)/shard_map/ppermute | solution.py:200
  70.1 0.0 collective-permute-done.4.refs_3_
  70.2 1.3 %collective-permute-start.15 = (bf16[512,128]{1,0:T(8,128)(2,1)}, bf16[512,128]{1,0:T(8,128)(2,1)S(1)}, u32[]{:S(2)}, u32[]{:S(2)}) collective-permute-start(bf16[512,128]{1,0:T(8,128)(2,1)} %shard_map.73.refs_6_), channel_id=1, source_target_pairs={{0,4},{2,6},{1,5},{3,7},{8,12},{10,14},{9,13},{11,15},{16,20},{18,... | collective-permute-start | bytes 393224 | tf_op jit(solution)/shard_map/ppermute | solution.py:200
  71.5 0.0 collective-permute-done.3.refs_2_
  71.5 1.2 %collective-permute-start.6 = (bf16[192,512]{1,0:T(8,128)(2,1)S(1)}, bf16[192,512]{1,0:T(8,128)(2,1)S(1)}, u32[]{:S(2)}, u32[]{:S(2)}) collective-permute-start(bf16[192,512]{1,0:T(8,128)(2,1)S(1)} %slice.103), channel_id=1, source_target_pairs={{0,8},{8,0},{16,24},{24,16},{1,9},{9,1},{17,25},{25,17},{2,10},{10... | collective-permute-start | bytes 589832 | tf_op jit(solution)/shard_map/ppermute | solution.py:23
  72.7 0.0 collective-permute-done.21.refs_3_
  72.8 0.9 collective-permute-start.5
  73.7 0.0 collective-permute-done.20.refs_2_
  73.7 0.8 collective-permute-start.23
  74.6 1.4 %collective-permute-start.22 = (bf16[192,512]{1,0:T(8,128)(2,1)S(1)}, bf16[192,512]{1,0:T(8,128)(2,1)S(1)}, u32[]{:S(2)}, u32[]{:S(2)}) collective-permute-start(bf16[192,512]{1,0:T(8,128)(2,1)S(1)} %slice.118), channel_id=1, source_target_pairs={{0,16},{8,24},{16,0},{24,8},{1,17},{9,25},{17,1},{25,9},{2,18},{10... | collective-permute-start | bytes 589832 | tf_op jit(solution)/shard_map/ppermute | solution.py:23
  76.0 3.1 %collective-permute-start.14 = (bf16[512,128]{1,0:T(8,128)(2,1)}, bf16[512,128]{1,0:T(8,128)(2,1)S(1)}, u32[]{:S(2)}, u32[]{:S(2)}) collective-permute-start(bf16[512,128]{1,0:T(8,128)(2,1)} %shard_map.73.refs_6_), channel_id=1, source_target_pairs={{0,2},{2,4},{4,6},{1,3},{3,5},{5,7},{8,10},{10,12},{12,14},{9,11},... | collective-permute-start | bytes 393224 | tf_op jit(solution)/shard_map/ppermute | solution.py:200
  79.0 2.8 %collective-permute-done.14.refs_7_ = bf16[512,128]{1,0:T(8,128)(2,1)S(1)} collective-permute-done((bf16[512,128]{1,0:T(8,128)(2,1)}, bf16[512,128]{1,0:T(8,128)(2,1)S(1)}, u32[]{:S(2)}, u32[]{:S(2)}) %collective-permute-start.14) | collective-permute-done | bytes 131104 | tf_op jit(solution)/shard_map/ppermute | solution.py:200
  81.9 0.6 copy-done.16
  82.5 0.1 copy-done.9
  82.6 0.7 copy-done.10
  83.2 14.5 %shard_map.74.att_ref = bf16[512,512]{1,0:T(8,128)(2,1)} custom-call(s32[3]{0:T(128)} %pad_add_fusion.where_ref, s32[8,16]{1,0:T(8,128)} %chosen_ref.1, bf16[512,2048]{1,0:T(8,128)(2,1)} %tok_ref.3, bf16[512,512]{1,0:T(8,128)(2,1)} %refs_0_.2, bf16[384,512]{1,0:T(8,128)(2,1)} %copy-done.5, bf16[384,512]{1,0:T(8,128)(2,1)} %copy-done.2, ...), custom_call_target="tpu_custom_call" | custom-call | tf_op jit(solution)/shard_map/pallas_call | solution.py:205
  97.8 0.0 collective-permute-done.22.refs_4_
  97.8 0.6 copy-done.11
  98.4 0.7 copy-done.12
  99.1 4.0 %shard_map.75 = (bf16[256,2048]{1,0:T(8,128)(2,1)}, bf16[256,2048]{1,0:T(8,128)(2,1)}) custom-call(s32[3]{0:T(128)} %pad_add_fusion.where_ref, bf16[512,512]{1,0:T(8,128)(2,1)} %shard_map.74.att_ref, bf16[512,512]{1,0:T(8,128)(2,1)} %refs_0_.3, bf16[384,512]{1,0:T(8,128)(2,1)} %copy-done.6, bf16[384,512]{1,0:T(8,128)(2,1)} %copy-done.4, ...), custom_call_target="tpu_custom_call" | custom-call | tf_op jit(solution)/shard_map/pallas_call | solution.py:228
  103.2 0.0 collective-permute-start.24
  103.2 2.9 %collective-permute-done.24.b_ref = bf16[256,2048]{1,0:T(8,128)(2,1)S(1)} collective-permute-done((bf16[256,2048]{1,0:T(8,128)(2,1)}, bf16[256,2048]{1,0:T(8,128)(2,1)S(1)}, u32[]{:S(2)}, u32[]{:S(2)}) %collective-permute-start.24) | collective-permute-done | bytes 1048608 | tf_op jit(solution)/shard_map/ppermute | solution.py:23
  106.0 1.0 copy-done
  107.0 3.2 %shard_map.76 = bf16[256,2048]{1,0:T(8,128)(2,1)} custom-call(bf16[256,2048]{1,0:T(8,128)(2,1)} %get-tuple-element.7.a_ref, bf16[256,2048]{1,0:T(8,128)(2,1)} %copy-done, f32[1,2048]{1,0:T(1,128)} %bitcast.4), custom_call_target="tpu_custom_call" | custom-call | tf_op jit(solution)/shard_map/pallas_call | solution.py:240
  (59 shorter events, 0.3 us)
Async XLA Ops:
  2.0 15.9 %collective-permute-start.9 = (bf16[128,128]{1,0:T(8,128)(2,1)S(1)}, bf16[128,128]{1,0:T(8,128)(2,1)S(1)}, u32[]{:S(2)}, u32[]{:S(2)}) collective-permute-start(bf16[128,128]{1,0:T(8,128)(2,1)S(1)} %fusion), channel_id=1, source_target_pairs={{0,6},{2,0},{4,2},{6,4},{1,7},{3,1},{5,3},{7,5},{8,14},{10,8},{12,... | collective-permute-start | bytes 98312 | tf_op jit(solution)/shard_map/ppermute | solution.py:19
  7.2 6.9 %collective-permute-start.8 = (bf16[128,128]{1,0:T(8,128)(2,1)S(1)}, bf16[128,128]{1,0:T(8,128)(2,1)S(1)}, u32[]{:S(2)}, u32[]{:S(2)}) collective-permute-start(bf16[128,128]{1,0:T(8,128)(2,1)S(1)} %fusion), channel_id=1, source_target_pairs={{0,4},{2,6},{4,0},{6,2},{1,5},{3,7},{5,1},{7,3},{8,12},{10,14},{12... | collective-permute-start | bytes 98312 | tf_op jit(solution)/shard_map/ppermute | solution.py:19
  7.2 6.8 %collective-permute-start.7 = (bf16[128,128]{1,0:T(8,128)(2,1)S(1)}, bf16[128,128]{1,0:T(8,128)(2,1)S(1)}, u32[]{:S(2)}, u32[]{:S(2)}) collective-permute-start(bf16[128,128]{1,0:T(8,128)(2,1)S(1)} %fusion), channel_id=1, source_target_pairs={{0,2},{2,4},{4,6},{6,0},{1,3},{3,5},{5,7},{7,1},{8,10},{10,12},{12... | collective-permute-start | bytes 98312 | tf_op jit(solution)/shard_map/ppermute | solution.py:19
  9.1 32.1 %collective-permute-start.19 = (bf16[128,512]{1,0:T(8,128)(2,1)S(1)}, bf16[128,512]{1,0:T(8,128)(2,1)S(1)}, u32[]{:S(2)}, u32[]{:S(2)}) collective-permute-start(bf16[128,512]{1,0:T(8,128)(2,1)S(1)} %constant_dynamic-slice_fusion), channel_id=1, source_target_pairs={{0,6},{2,0},{4,2},{6,4},{1,7},{3,1},{5,3},{7,5},{8,14},{10,8},{12,... | collective-permute-start | bytes 393224 | tf_op jit(solution)/shard_map/ppermute | solution.py:19
  12.0 28.6 %collective-permute-start.18 = (bf16[128,512]{1,0:T(8,128)(2,1)S(1)}, bf16[128,512]{1,0:T(8,128)(2,1)S(1)}, u32[]{:S(2)}, u32[]{:S(2)}) collective-permute-start(bf16[128,512]{1,0:T(8,128)(2,1)S(1)} %constant_dynamic-slice_fusion), channel_id=1, source_target_pairs={{0,4},{2,6},{4,0},{6,2},{1,5},{3,7},{5,1},{7,3},{8,12},{10,14},{12... | collective-permute-start | bytes 393224 | tf_op jit(solution)/shard_map/ppermute | solution.py:19
  14.0 26.0 %collective-permute-start.17 = (bf16[128,512]{1,0:T(8,128)(2,1)S(1)}, bf16[128,512]{1,0:T(8,128)(2,1)S(1)}, u32[]{:S(2)}, u32[]{:S(2)}) collective-permute-start(bf16[128,512]{1,0:T(8,128)(2,1)S(1)} %constant_dynamic-slice_fusion), channel_id=1, source_target_pairs={{0,2},{2,4},{4,6},{6,0},{1,3},{3,5},{5,7},{7,1},{8,10},{10,12},{12... | collective-permute-start | bytes 393224 | tf_op jit(solution)/shard_map/ppermute | solution.py:19
  14.1 24.3 %collective-permute-start.2 = (bf16[128,512]{1,0:T(8,128)(2,1)S(1)}, bf16[128,512]{1,0:T(8,128)(2,1)S(1)}, u32[]{:S(2)}, u32[]{:S(2)}) collective-permute-start(bf16[128,512]{1,0:T(8,128)(2,1)S(1)} %constant_dynamic-slice_fusion.1), channel_id=1, source_target_pairs={{0,6},{2,0},{4,2},{6,4},{1,7},{3,1},{5,3},{7,5},{8,14},{10,8},{12,... | collective-permute-start | bytes 393224 | tf_op jit(solution)/shard_map/ppermute | solution.py:19
  17.9 8.9 %collective-permute-start = (bf16[128,512]{1,0:T(8,128)(2,1)S(1)}, bf16[128,512]{1,0:T(8,128)(2,1)S(1)}, u32[]{:S(2)}, u32[]{:S(2)}) collective-permute-start(bf16[128,512]{1,0:T(8,128)(2,1)S(1)} %constant_dynamic-slice_fusion.1), channel_id=1, source_target_pairs={{0,2},{2,4},{4,6},{6,0},{1,3},{3,5},{5,7},{7,1},{8,10},{10,12},{12... | collective-permute-start | bytes 393224 | tf_op jit(solution)/shard_map/ppermute | solution.py:19
  18.0 47.1 %copy-start.13 = (bf16[384,128]{1,0:T(8,128)(2,1)}, bf16[384,128]{1,0:T(8,128)(2,1)S(1)}, u32[]{:S(2)}) copy-start(bf16[384,128]{1,0:T(8,128)(2,1)S(1)} %constant_dynamic-update-slice_fusion.refs_1_) | copy-start | bytes 294916
  26.8 10.0 %collective-permute-start.1 = (bf16[128,512]{1,0:T(8,128)(2,1)S(1)}, bf16[128,512]{1,0:T(8,128)(2,1)S(1)}, u32[]{:S(2)}, u32[]{:S(2)}) collective-permute-start(bf16[128,512]{1,0:T(8,128)(2,1)S(1)} %constant_dynamic-slice_fusion.1), channel_id=1, source_target_pairs={{0,4},{2,6},{4,0},{6,2},{1,5},{3,7},{5,1},{7,3},{8,12},{10,14},{12... | collective-permute-start | bytes 393224 | tf_op jit(solution)/shard_map/ppermute | solution.py:19
  36.8 6.0 %collective-permute-start.11 = (bf16[384,128]{1,0:T(8,128)(2,1)S(1)}, bf16[384,128]{1,0:T(8,128)(2,1)S(1)}, u32[]{:S(2)}, u32[]{:S(2)}) collective-permute-start(bf16[384,128]{1,0:T(8,128)(2,1)S(1)} %constant_dynamic-update-slice_fusion.refs_1_), channel_id=1, source_target_pairs={{0,16},{8,24},{16,0},{24,8},{1,17},{9,25},{17,1},{25,9},{2,18},{10... | collective-permute-start | bytes 294920 | tf_op jit(solution)/shard_map/ppermute | solution.py:23
  38.4 6.0 %collective-permute-start.10 = (bf16[384,128]{1,0:T(8,128)(2,1)S(1)}, bf16[384,128]{1,0:T(8,128)(2,1)S(1)}, u32[]{:S(2)}, u32[]{:S(2)}) collective-permute-start(bf16[384,128]{1,0:T(8,128)(2,1)S(1)} %constant_dynamic-update-slice_fusion.refs_1_), channel_id=1, source_target_pairs={{0,8},{8,0},{16,24},{24,16},{1,9},{9,1},{17,25},{25,17},{2,10},{10... | collective-permute-start | bytes 294920 | tf_op jit(solution)/shard_map/ppermute | solution.py:23
  40.0 31.5 %copy-start.5 = (bf16[384,512]{1,0:T(8,128)(2,1)}, bf16[384,512]{1,0:T(8,128)(2,1)S(1)}, u32[]{:S(2)}) copy-start(bf16[384,512]{1,0:T(8,128)(2,1)S(1)} %slice_dynamic-update-slice_fusion.6.refs_1_) | copy-start | bytes 1179652
  40.0 30.2 %collective-permute-start.4 = (bf16[384,512]{1,0:T(8,128)(2,1)S(1)}, bf16[384,512]{1,0:T(8,128)(2,1)S(1)}, u32[]{:S(2)}, u32[]{:S(2)}) collective-permute-start(bf16[384,512]{1,0:T(8,128)(2,1)S(1)} %slice_dynamic-update-slice_fusion.6.refs_1_), channel_id=1, source_target_pairs={{0,16},{8,24},{16,0},{24,8},{1,17},{9,25},{17,1},{25,9},{2,18},{10... | collective-permute-start | bytes 1179656 | tf_op jit(solution)/shard_map/ppermute | solution.py:23
  40.6 30.9 %collective-permute-start.3 = (bf16[384,512]{1,0:T(8,128)(2,1)S(1)}, bf16[384,512]{1,0:T(8,128)(2,1)S(1)}, u32[]{:S(2)}, u32[]{:S(2)}) collective-permute-start(bf16[384,512]{1,0:T(8,128)(2,1)S(1)} %slice_dynamic-update-slice_fusion.6.refs_1_), channel_id=1, source_target_pairs={{0,8},{8,0},{16,24},{24,16},{1,9},{9,1},{17,25},{25,17},{2,10},{10... | collective-permute-start | bytes 1179656 | tf_op jit(solution)/shard_map/ppermute | solution.py:23
  41.2 32.5 %copy-start.6 = (bf16[384,512]{1,0:T(8,128)(2,1)}, bf16[384,512]{1,0:T(8,128)(2,1)S(1)}, u32[]{:S(2)}) copy-start(bf16[384,512]{1,0:T(8,128)(2,1)S(1)} %slice_dynamic-update-slice_fusion.refs_1_) | copy-start | bytes 1179652
  41.2 31.5 %collective-permute-start.21 = (bf16[384,512]{1,0:T(8,128)(2,1)S(1)}, bf16[384,512]{1,0:T(8,128)(2,1)S(1)}, u32[]{:S(2)}, u32[]{:S(2)}) collective-permute-start(bf16[384,512]{1,0:T(8,128)(2,1)S(1)} %slice_dynamic-update-slice_fusion.refs_1_), channel_id=1, source_target_pairs={{0,16},{8,24},{16,0},{24,8},{1,17},{9,25},{17,1},{25,9},{2,18},{10... | collective-permute-start | bytes 1179656 | tf_op jit(solution)/shard_map/ppermute | solution.py:23
  42.8 22.2 %copy-start.7 = (bf16[384,128]{1,0:T(8,128)(2,1)}, bf16[384,128]{1,0:T(8,128)(2,1)S(1)}, u32[]{:S(2)}) copy-start(bf16[384,128]{1,0:T(8,128)(2,1)S(1)} %collective-permute-done.11.refs_3_) | copy-start | bytes 294916
  42.8 30.9 %collective-permute-start.20 = (bf16[384,512]{1,0:T(8,128)(2,1)S(1)}, bf16[384,512]{1,0:T(8,128)(2,1)S(1)}, u32[]{:S(2)}, u32[]{:S(2)}) collective-permute-start(bf16[384,512]{1,0:T(8,128)(2,1)S(1)} %slice_dynamic-update-slice_fusion.refs_1_), channel_id=1, source_target_pairs={{0,8},{8,0},{16,24},{24,16},{1,9},{9,1},{17,25},{25,17},{2,10},{10... | collective-permute-start | bytes 1179656 | tf_op jit(solution)/shard_map/ppermute | solution.py:23
  44.3 20.7 %copy-start.8 = (bf16[384,128]{1,0:T(8,128)(2,1)}, bf16[384,128]{1,0:T(8,128)(2,1)S(1)}, u32[]{:S(2)}) copy-start(bf16[384,128]{1,0:T(8,128)(2,1)S(1)} %collective-permute-done.10.refs_2_) | copy-start | bytes 294916
  44.3 16.6 %collective-permute-start.13 = (bf16[192,128]{1,0:T(8,128)(2,1)S(1)}, bf16[192,128]{1,0:T(8,128)(2,1)S(1)}, u32[]{:S(2)}, u32[]{:S(2)}) collective-permute-start(bf16[192,128]{1,0:T(8,128)(2,1)S(1)} %slice.111), channel_id=1, source_target_pairs={{0,8},{8,0},{16,24},{24,16},{1,9},{9,1},{17,25},{25,17},{2,10},{10... | collective-permute-start | bytes 147464 | tf_op jit(solution)/shard_map/ppermute | solution.py:23
  60.9 4.1 %copy-start.17 = (bf16[192,128]{1,0:T(8,128)(2,1)}, bf16[192,128]{1,0:T(8,128)(2,1)S(1)}, u32[]{:S(2)}) copy-start(bf16[192,128]{1,0:T(8,128)(2,1)S(1)} %collective-permute-done.13.refs_5_) | copy-start | bytes 147460
  60.9 4.1 %collective-permute-start.12 = (bf16[192,128]{1,0:T(8,128)(2,1)S(1)}, bf16[192,128]{1,0:T(8,128)(2,1)S(1)}, u32[]{:S(2)}, u32[]{:S(2)}) collective-permute-start(bf16[192,128]{1,0:T(8,128)(2,1)S(1)} %slice.110), channel_id=1, source_target_pairs={{0,16},{8,24},{16,0},{24,8},{1,17},{9,25},{17,1},{25,9},{2,18},{10... | collective-permute-start | bytes 147464 | tf_op jit(solution)/shard_map/ppermute | solution.py:23
  65.1 0.6 copy-start.18
  68.8 5.7 %collective-permute-start.16 = (bf16[512,128]{1,0:T(8,128)(2,1)}, bf16[512,128]{1,0:T(8,128)(2,1)S(1)}, u32[]{:S(2)}, u32[]{:S(2)}) collective-permute-start(bf16[512,128]{1,0:T(8,128)(2,1)} %shard_map.73.refs_6_), channel_id=1, source_target_pairs={{0,6},{1,7},{8,14},{9,15},{16,22},{17,23},{24,30},{25,31}} | collective-permute-start | bytes 393224 | tf_op jit(solution)/shard_map/ppermute | solution.py:200
  70.1 11.7 %copy-start.1 = (bf16[384,512]{1,0:T(8,128)(2,1)}, bf16[384,512]{1,0:T(8,128)(2,1)S(1)}, u32[]{:S(2)}) copy-start(bf16[384,512]{1,0:T(8,128)(2,1)S(1)} %collective-permute-done.4.refs_3_) | copy-start | bytes 1179652
  70.2 5.8 %collective-permute-start.15 = (bf16[512,128]{1,0:T(8,128)(2,1)}, bf16[512,128]{1,0:T(8,128)(2,1)S(1)}, u32[]{:S(2)}, u32[]{:S(2)}) collective-permute-start(bf16[512,128]{1,0:T(8,128)(2,1)} %shard_map.73.refs_6_), channel_id=1, source_target_pairs={{0,4},{2,6},{1,5},{3,7},{8,12},{10,14},{9,13},{11,15},{16,20},{18,... | collective-permute-start | bytes 393224 | tf_op jit(solution)/shard_map/ppermute | solution.py:200
  71.5 10.4 %copy-start.2 = (bf16[384,512]{1,0:T(8,128)(2,1)}, bf16[384,512]{1,0:T(8,128)(2,1)S(1)}, u32[]{:S(2)}) copy-start(bf16[384,512]{1,0:T(8,128)(2,1)S(1)} %collective-permute-done.3.refs_2_) | copy-start | bytes 1179652
  71.5 10.3 %collective-permute-start.6 = (bf16[192,512]{1,0:T(8,128)(2,1)S(1)}, bf16[192,512]{1,0:T(8,128)(2,1)S(1)}, u32[]{:S(2)}, u32[]{:S(2)}) collective-permute-start(bf16[192,512]{1,0:T(8,128)(2,1)S(1)} %slice.103), channel_id=1, source_target_pairs={{0,8},{8,0},{16,24},{24,16},{1,9},{9,1},{17,25},{25,17},{2,10},{10... | collective-permute-start | bytes 589832 | tf_op jit(solution)/shard_map/ppermute | solution.py:23
  72.8 25.0 %copy-start.3 = (bf16[384,512]{1,0:T(8,128)(2,1)}, bf16[384,512]{1,0:T(8,128)(2,1)S(1)}, u32[]{:S(2)}) copy-start(bf16[384,512]{1,0:T(8,128)(2,1)S(1)} %collective-permute-done.21.refs_3_) | copy-start | bytes 1179652
  72.8 9.1 %collective-permute-start.5 = (bf16[192,512]{1,0:T(8,128)(2,1)S(1)}, bf16[192,512]{1,0:T(8,128)(2,1)S(1)}, u32[]{:S(2)}, u32[]{:S(2)}) collective-permute-start(bf16[192,512]{1,0:T(8,128)(2,1)S(1)} %slice.102), channel_id=1, source_target_pairs={{0,16},{8,24},{16,0},{24,8},{1,17},{9,25},{17,1},{25,9},{2,18},{10... | collective-permute-start | bytes 589832 | tf_op jit(solution)/shard_map/ppermute | solution.py:23
  73.7 24.0 %copy-start.4 = (bf16[384,512]{1,0:T(8,128)(2,1)}, bf16[384,512]{1,0:T(8,128)(2,1)S(1)}, u32[]{:S(2)}) copy-start(bf16[384,512]{1,0:T(8,128)(2,1)S(1)} %collective-permute-done.20.refs_2_) | copy-start | bytes 1179652
  73.7 24.0 %collective-permute-start.23 = (bf16[192,512]{1,0:T(8,128)(2,1)S(1)}, bf16[192,512]{1,0:T(8,128)(2,1)S(1)}, u32[]{:S(2)}, u32[]{:S(2)}) collective-permute-start(bf16[192,512]{1,0:T(8,128)(2,1)S(1)} %slice.119), channel_id=1, source_target_pairs={{0,8},{8,0},{16,24},{24,16},{1,9},{9,1},{17,25},{25,17},{2,10},{10... | collective-permute-start | bytes 589832 | tf_op jit(solution)/shard_map/ppermute | solution.py:23
  74.6 7.3 %copy-start.14 = (bf16[512,128]{1,0:T(8,128)(2,1)}, bf16[512,128]{1,0:T(8,128)(2,1)S(1)}, u32[]{:S(2)}) copy-start(bf16[512,128]{1,0:T(8,128)(2,1)S(1)} %collective-permute-done.16.refs_9_) | copy-start | bytes 393220
  74.6 23.2 %collective-permute-start.22 = (bf16[192,512]{1,0:T(8,128)(2,1)S(1)}, bf16[192,512]{1,0:T(8,128)(2,1)S(1)}, u32[]{:S(2)}, u32[]{:S(2)}) collective-permute-start(bf16[192,512]{1,0:T(8,128)(2,1)S(1)} %slice.118), channel_id=1, source_target_pairs={{0,16},{8,24},{16,0},{24,8},{1,17},{9,25},{17,1},{25,9},{2,18},{10... | collective-permute-start | bytes 589832 | tf_op jit(solution)/shard_map/ppermute | solution.py:23
  76.0 5.9 %copy-start.15 = (bf16[512,128]{1,0:T(8,128)(2,1)}, bf16[512,128]{1,0:T(8,128)(2,1)S(1)}, u32[]{:S(2)}) copy-start(bf16[512,128]{1,0:T(8,128)(2,1)S(1)} %collective-permute-done.15.refs_8_) | copy-start | bytes 393220
  76.0 5.9 %collective-permute-start.14 = (bf16[512,128]{1,0:T(8,128)(2,1)}, bf16[512,128]{1,0:T(8,128)(2,1)S(1)}, u32[]{:S(2)}, u32[]{:S(2)}) collective-permute-start(bf16[512,128]{1,0:T(8,128)(2,1)} %shard_map.73.refs_6_), channel_id=1, source_target_pairs={{0,2},{2,4},{4,6},{1,3},{3,5},{5,7},{8,10},{10,12},{12,14},{9,11},... | collective-permute-start | bytes 393224 | tf_op jit(solution)/shard_map/ppermute | solution.py:200
  81.8 0.7 copy-start.16
  81.8 0.7 copy-start.9
  82.6 0.7 copy-start.10
  97.8 0.7 copy-start.11
  98.4 0.7 copy-start.12
  103.2 2.9 %collective-permute-start.24 = (bf16[256,2048]{1,0:T(8,128)(2,1)}, bf16[256,2048]{1,0:T(8,128)(2,1)S(1)}, u32[]{:S(2)}, u32[]{:S(2)}) collective-permute-start(bf16[256,2048]{1,0:T(8,128)(2,1)} %get-tuple-element.8), channel_id=1, source_target_pairs={{0,1},{1,0},{2,3},{3,2},{4,5},{5,4},{6,7},{7,6},{8,9},{9,8},{10,11... | collective-permute-start | bytes 3145736 | tf_op jit(solution)/shard_map/ppermute | solution.py:23
  106.0 1.0 copy-start

commit v2 on v1

--- a/solution.py
+++ b/solution.py
@@ -7,6 +7,7 @@
 from jax.experimental.pallas import tpu as pltpu
 from jax.sharding import PartitionSpec as P
 
+
 HEAD_WIDTH = 64
 BLOCK_LENGTH = 64
 ALIGN = 16
@@ -23,51 +24,47 @@
     return lax.ppermute(x, axis, [(i, i ^ bit) for i in range(count)])
 
 
-def spread(w, kv_count, dp_count):
+def piece_of(w, dp_count):
     rows = w.shape[0] // dp_count
-    half = rows // 2
-    dp = lax.axis_index("dp")
-    piece = lax.dynamic_slice_in_dim(w, dp * rows, rows, axis=0)
-    got = [shift(piece, "kv", s, kv_count) for s in range(1, kv_count)]
-    mine = jnp.concatenate([g[:half] for g in got] + [g[half:] for g in got], axis=0)
-    cut = half * (kv_count - 1)
-    across = swap(mine, "dp", 1, dp_count)
-    along = swap(mine, "dp", 2, dp_count)
-    far_top = swap(across[:cut], "dp", 2, dp_count)
-    far_low = swap(along[cut:], "dp", 1, dp_count)
-    return [w, mine, across, along, far_top, far_low]
-
-
-def place(refs, dest, kv, dp, kv_count, dp_count):
+    return lax.dynamic_slice_in_dim(w, lax.axis_index("dp") * rows, rows, axis=0)
+
+
+def along_kv(piece, kv_count):
+    got = []
+    for s in range(1, kv_count):
+        got.append(shift(piece, "kv", s, kv_count))
+    return got
+
+
+def across_dp(w, got, dp_count):
+    mine = jnp.concatenate(got, axis=0)
+    parts = [w, mine]
+    for bits in range(1, dp_count):
+        parts.append(swap(mine, "dp", bits, dp_count))
+    return parts
+
+
+def place(refs, dest, kv, dp, kv_count):
     if len(refs) == 1:
         dest[...] = refs[0][...].reshape(dest.shape)
         return
-    own, mine, across, along, far_top, far_low = refs
+    own = refs[0]
     dest[pl.ds(kv, 1)] = own[...][None]
-    rows = own.shape[0] // dp_count
-    half = rows // 2
-    cut = half * (kv_count - 1)
+    rows = own.shape[0] // (len(refs) - 1)
     for s in range(1, kv_count):
         source = lax.rem(kv - s + kv_count, kv_count)
-        at = half * (s - 1)
-        for h in range(2):
-            for bits, ref, base in (
-                (0, mine, h * cut),
-                (1, across, h * cut),
-                (2, along, h * cut),
-                (3, (far_top, far_low)[h], 0),
-            ):
-                first = pl.multiple_of((dp ^ bits) * rows + h * half, half)
-                dest[pl.ds(source, 1), pl.ds(first, half)] = ref[pl.ds(base + at, half)][None]
-
-
-def attend_kernel(where_ref, chosen_ref, tok_ref, *refs, n_weights, n_rows, kv_count, dp_count, heads):
+        for bits, ref in enumerate(refs[1:]):
+            first = pl.multiple_of((dp ^ bits) * rows, rows)
+            dest[pl.ds(source, 1), pl.ds(first, rows)] = ref[(s - 1) * rows:s * rows][None]
+
+
+def attend_kernel(where_ref, chosen_ref, tok_ref, *refs, n_weights, n_rows, kv_count, heads):
     w_refs = refs[:n_weights]
     row_refs = refs[n_weights:n_weights + n_rows]
     out_ref, w_full, kv_full, q_full, picked = refs[n_weights + n_rows:]
     kv = where_ref[0]
     dp = where_ref[1]
-    place(w_refs, w_full, kv, dp, kv_count, dp_count)
+    place(w_refs, w_full, kv, dp, kv_count)
     if n_rows == 1:
         kv_full[...] = row_refs[0][...]
     else:
@@ -130,13 +127,13 @@
     lax.fori_loop(0, blocks, one_block, 0)
 
 
-def project_kernel(where_ref, att_ref, *refs, n_weights, kv_count, dp_count):
+def project_kernel(where_ref, att_ref, *refs, n_weights, kv_count):
     w_refs = refs[:n_weights]
     mine_ref, other_ref, w_full = refs[n_weights:]
     tp = where_ref[2]
     half = mine_ref.shape[0]
     width = w_full.shape[2]
-    place(w_refs, w_full, where_ref[0], where_ref[1], kv_count, dp_count)
+    place(w_refs, w_full, where_ref[0], where_ref[1], kv_count)
     for out, which in ((other_ref, 1 - tp), (mine_ref, tp)):
         rows = att_ref[pl.ds(pl.multiple_of(which * half, half), half)]
         for k in range(w_full.shape[0]):
@@ -151,7 +148,7 @@
     out_ref[...] = (mixed * scale * gain_ref[...]).astype(BF16)
 
 
-def per_device(tokens, chosen, query_weight, key_matrix, value_matrix, out_weight, out_gain):
+def layer(tokens, chosen, query_weight, key_matrix, value_matrix, out_weight, out_gain):
     kv_count = lax.axis_size("kv")
     dp_count = lax.axis_size("dp")
     tp_count = lax.axis_size("tp")
@@ -163,43 +160,42 @@
     heads = query_weight.shape[1] // HEAD_WIDTH
     shard = query_weight.shape[0]
     direct = (
-        dp_count == 4
+        dp_count & (dp_count - 1) == 0
+        and dp_count <= 8
         and kv_count <= 8
-        and shard % (2 * dp_count * ALIGN) == 0
+        and shard % (dp_count * ALIGN) == 0
         and out_weight.shape[1] % 128 == 0
     )
-    pair_shard = jnp.concatenate([key_matrix, value_matrix], axis=1)
     if direct:
-        pair_parts = spread(pair_shard, kv_count, dp_count)
-        q_parts = spread(query_weight, kv_count, dp_count)
-        o_parts = spread(out_weight, kv_count, dp_count)
-        pair_kernel = functools.partial(
-            pair_project, n_weights=len(pair_parts), kv_count=kv_count, dp_count=dp_count
-        )
+        pair_piece = jnp.concatenate(
+            [piece_of(key_matrix, dp_count), piece_of(value_matrix, dp_count)], axis=1
+        )
+        pair_line = lax.all_gather(pair_piece, "kv", axis=0)
+        q_piece, pair_line = lax.optimization_barrier((piece_of(query_weight, dp_count), pair_line))
+        q_got = along_kv(q_piece, kv_count)
+        pair_whole = lax.all_gather(pair_line, "dp", axis=0)
     else:
-        pair_parts = [lax.all_gather(pair_shard, "kv", axis=0, tiled=True)]
+        pair_shard = jnp.concatenate([key_matrix, value_matrix], axis=1)
+        pair_whole = lax.all_gather(pair_shard, "kv", axis=0)[None]
         q_parts = [lax.all_gather(query_weight, "kv", axis=0, tiled=True)]
         o_parts = [lax.all_gather(out_weight, "kv", axis=1, tiled=True)]
-        pair_kernel = functools.partial(
-            pair_project, n_weights=1, kv_count=kv_count, dp_count=dp_count
-        )
     vmem = pl.BlockSpec(memory_space=pltpu.VMEM)
     smem = pl.BlockSpec(memory_space=pltpu.SMEM)
-    pair_width = pair_shard.shape[1]
+    pair_width = pair_whole.shape[-1]
     pairs = pl.pallas_call(
-        pair_kernel,
+        pair_project,
         out_shape=jax.ShapeDtypeStruct((tok_rows, pair_width), BF16),
-        in_specs=[smem, vmem] + [vmem] * len(pair_parts),
+        in_specs=[vmem, vmem],
         out_specs=vmem,
-        scratch_shapes=[pltpu.VMEM((kv_count, shard, pair_width), BF16)]
-        if direct
-        else [pltpu.VMEM((1, model, pair_width), BF16)],
-    )(where, tokens, *pair_parts)
+        scratch_shapes=[pltpu.VMEM((model, pair_width), BF16)],
+    )(tokens, pair_whole)
     if direct:
-        row_parts = [pairs] + [
-            lax.ppermute(pairs, "kv", [(i, i + s) for i in range(kv_count - s)])
-            for s in range(1, kv_count)
-        ]
+        row_parts = [pairs]
+        for s in range(1, kv_count):
+            row_parts.append(lax.ppermute(pairs, "kv", [(i, i + s) for i in range(kv_count - s)]))
+        q_parts = across_dp(query_weight, q_got, dp_count)
+        o_got = along_kv(piece_of(out_weight, dp_count), kv_count)
+        o_parts = across_dp(out_weight, o_got, dp_count)
     else:
         row_parts = [lax.all_gather(pairs, "kv", axis=0, tiled=True)]
     attended = pl.pallas_call(
@@ -208,7 +204,6 @@
             n_weights=len(q_parts),
             n_rows=len(row_parts),
             kv_count=kv_count,
-            dp_count=dp_count,
             heads=heads,
         ),
         out_shape=jax.ShapeDtypeStruct((tok_rows, heads * HEAD_WIDTH), BF16),
@@ -220,6 +215,11 @@
             pltpu.VMEM((tok_rows, heads * HEAD_WIDTH), BF16),
             pltpu.VMEM((chosen.shape[1] * BLOCK_LENGTH, pair_width), BF16),
         ],
+        cost_estimate=pl.CostEstimate(
+            flops=64 * tok_rows * model * heads * HEAD_WIDTH,
+            bytes_accessed=2 * tok_rows * model,
+            transcendentals=0,
+        ),
     )(where, chosen, tokens, *q_parts, *row_parts)
     out_rows = tok_rows // tp_count
     head_rows, out_cols = out_weight.shape
@@ -227,7 +227,7 @@
     piece = jax.ShapeDtypeStruct((out_rows, columns), BF16)
     mine, other = pl.pallas_call(
         functools.partial(
-            project_kernel, n_weights=len(o_parts), kv_count=kv_count, dp_count=dp_count
+            project_kernel, n_weights=len(o_parts), kv_count=kv_count
         ),
         out_shape=(piece, piece),
         in_specs=[smem, vmem] + [vmem] * len(o_parts),
@@ -245,12 +245,13 @@
     )(mine, theirs, out_gain.reshape(1, -1))
 
 
-def pair_project(where_ref, tok_ref, *refs, n_weights, kv_count, dp_count):
-    w_refs = refs[:n_weights]
-    out_ref, w_full = refs[n_weights:]
-    place(w_refs, w_full, where_ref[0], where_ref[1], kv_count, dp_count)
-    whole = w_full[...].reshape(-1, w_full.shape[-1])
-    out_ref[...] = jnp.dot(tok_ref[...], whole, preferred_element_type=F32).astype(BF16)
+def pair_project(tok_ref, w_ref, out_ref, w_full):
+    dp_count, kv_count, rows = w_ref.shape[:3]
+    for k in range(kv_count):
+        for d in range(dp_count):
+            at = (k * dp_count + d) * rows
+            w_full[at:at + rows] = w_ref[d, k]
+    out_ref[...] = jnp.dot(tok_ref[...], w_full[...], preferred_element_type=F32).astype(BF16)
 
 
 def solution(mesh):
@@ -264,7 +265,7 @@
         P(),
     )
     return jax.shard_map(
-        per_device,
+        layer,
         mesh=mesh,
         in_specs=placed,
         out_specs=P(("dp", "kv", "tp"), None),

time: 111 us -> 95 us (0.86)
  waiting for transfers between devices: 37.5 us -> 12.5 us
  blocking collectives: 0 us -> 24.7 us
  starting transfers between devices: 37.6 us -> 24.8 us
  local copies, waits for them, and re-layouts: 8.22 us -> 6.79 us
    all_gather x0 -> x2, blocking collectives: none -> 24.7 us  [the longest x1 13.9 us: layer(): pair_line = lax.all_gather(pair_piece, 'kv', axis=0)]
    ppermute x9 -> x6, waiting for transfers between devices: 14.5 us -> 0.02 us  [shift(): return lax.ppermute(x, axis, [(i, (i + by) % count) for i in range(count)])]
    ppermute x9 -> x6, starting transfers between devices: 18.4 us -> 7.87 us  [shift(): return lax.ppermute(x, axis, [(i, (i + by) % count) for i in range(count)])]
    ppermute x13 -> x7, waiting for transfers between devices: 20.2 us -> 11.2 us  [swap(): return lax.ppermute(x, axis, [(i, i ^ bit) for i in range(count)])]
    ppermute x13 -> x7, starting transfers between devices: 13.6 us -> 7.78 us  [swap(): return lax.ppermute(x, axis, [(i, i ^ bit) for i in range(count)])]
    ppermute x3, starting transfers between devices: 5.64 us -> 9.14 us  [layer(): lax.ppermute(pairs, 'kv', [(i, i + s) for i in range(kv_count - s)])]
    unnamed x55 -> x28, local copies, waits for them, and re-layouts: 6.31 us -> 4.08 us
    ppermute x3, waiting for transfers between devices: 2.82 us -> 1.3 us  [layer(): lax.ppermute(pairs, 'kv', [(i, i + s) for i in range(kv_count - s)])]
  transfers between devices with their start and end apart: 25 -> 16, of which waited for: 6 -> 5; matrix products, arithmetic and copies ran while one was open for 3% -> 2% of each run, Pallas kernels for 16% -> 19%
where the time goes in v2:
time: 95 us; the launch traced here: 94.6 us
  Pallas kernels  25 us (26%)
  starting transfers between devices  24.8 us (26%)
  blocking collectives  24.7 us (26%)
  waiting for transfers between devices  12.5 us (13%)
  local copies, waits for them, and re-layouts  6.79 us (7%)
    pallas_call x1, Pallas kernels, layer(): pl.pallas_call(functools.partial(attend_kernel, n_weights=len(q_parts), n...  14.6 us
    all_gather x1, blocking collectives, layer(): pair_line = lax.all_gather(pair_piece, 'kv', axis=0)  13.9 us
    ppermute x7, waiting for transfers between devices, swap(): return lax.ppermute(x, axis, [(i, i ^ bit) for i in range(count)])  11.2 us
    all_gather x1, blocking collectives, layer(): pair_whole = lax.all_gather(pair_line, 'dp', axis=0)  10.8 us
    ppermute x3, starting transfers between devices, layer(): lax.ppermute(pairs, 'kv', [(i, i + s) for i in range(kv_count - s)])  9.14 us
    ppermute x6, starting transfers between devices, shift(): return lax.ppermute(x, axis, [(i, (i + by) % count) for i in range(count)])  7.87 us
    ppermute x7, starting transfers between devices, swap(): return lax.ppermute(x, axis, [(i, i ^ bit) for i in range(count)])  7.78 us
    unnamed x28, local copies, waits for them, and re-layouts  4.08 us
  transfers between devices with their start and end apart: 16, of which 5 were waited for; matrix products, arithmetic and copies ran while one was open for 2% of the time, Pallas kernels for 19%

profile of v2, /device:TPU:0, one launch (start us, length us, event | category | flops | bytes accessed | tf_op | source)
XLA Modules:
  0.0 94.6 jit_solution(16195005364897762075)
XLA Ops:
  0.0 0.7 constant_dynamic-slice_fusion.1
  0.7 13.9 %all-gather = bf16[512,128]{0,1:T(8,128)(2,1)S(1)} all-gather(bf16[128,128]{0,1:T(8,128)(2,1)S(1)} %pad_maximum_fusion), channel_id=2, replica_groups=mesh['dp'=4,'kv'=4,'tp'=2] {'kv'}, dimensions={0}, use_global_device_ids=true | all-gather | bytes 163840 | tf_op jit(solution)/shard_map/all_gather | solution.py:173
  14.7 0.1 copy.9
  14.8 0.9 constant_dynamic-slice_fusion.3
  15.7 2.5 %collective-permute-start.2 = (bf16[128,512]{1,0:T(8,128)(2,1)S(1)}, bf16[128,512]{1,0:T(8,128)(2,1)S(1)}, u32[]{:S(2)}, u32[]{:S(2)}) collective-permute-start(bf16[128,512]{1,0:T(8,128)(2,1)S(1)} %constant_dynamic-slice_fusion.3), channel_id=1, source_target_pairs={{0,6},{2,0},{4,2},{6,4},{1,7},{3,1},{5,3},{7,5},{8,14},{10,8},{12,... | collective-permute-start | bytes 393224 | tf_op jit(solution)/shard_map/ppermute | solution.py:20
  18.2 0.9 collective-permute-start.1
  19.1 0.0 collective-permute-start
  19.1 0.9 constant_dynamic-slice_fusion
  20.0 3.9 %collective-permute-start.11 = (bf16[128,512]{1,0:T(8,128)(2,1)S(1)}, bf16[128,512]{1,0:T(8,128)(2,1)S(1)}, u32[]{:S(2)}, u32[]{:S(2)}) collective-permute-start(bf16[128,512]{1,0:T(8,128)(2,1)S(1)} %constant_dynamic-slice_fusion), channel_id=1, source_target_pairs={{0,6},{2,0},{4,2},{6,4},{1,7},{3,1},{5,3},{7,5},{8,14},{10,8},{12,... | collective-permute-start | bytes 393224 | tf_op jit(solution)/shard_map/ppermute | solution.py:20
  23.9 0.3 collective-permute-start.10
  24.1 10.8 %all-gather.1 = bf16[16,128,128]{2,1,0:T(8,128)(2,1)} all-gather(bf16[4,128,128]{2,1,0:T(8,128)(2,1)S(1)} %bitcast.7), channel_id=3, replica_groups=mesh['dp'=4,'kv'=4,'tp'=2] {'dp'}, dimensions={0}, use_global_device_ids=true | all-gather | bytes 655360 | tf_op jit(solution)/shard_map/all_gather | solution.py:176
  34.9 3.1 %shard_map.73.refs_5_ = bf16[512,128]{1,0:T(8,128)(2,1)} custom-call(bf16[512,2048]{1,0:T(8,128)(2,1)} %tok_ref.3, bf16[4,4,128,128]{3,2,1,0:T(8,128)(2,1)} %bitcast.6), custom_call_target="tpu_custom_call" | custom-call | tf_op jit(solution)/shard_map/pallas_call | solution.py:185
  38.0 0.0 collective-permute-done
  38.0 0.4 collective-permute-start.9
  38.4 0.0 collective-permute-done.1
  38.4 5.4 %collective-permute-start.8 = (bf16[512,128]{1,0:T(8,128)(2,1)}, bf16[512,128]{1,0:T(8,128)(2,1)S(1)}, u32[]{:S(2)}, u32[]{:S(2)}) collective-permute-start(bf16[512,128]{1,0:T(8,128)(2,1)} %shard_map.73.refs_5_), channel_id=1, source_target_pairs={{0,6},{1,7},{8,14},{9,15},{16,22},{17,23},{24,30},{25,31}} | collective-permute-start | bytes 393224 | tf_op jit(solution)/shard_map/ppermute | solution.py:195
  43.8 0.0 collective-permute-done.2
  43.8 0.0 copy-start.5
  43.8 1.5 %collective-permute-start.5 = (bf16[384,512]{1,0:T(8,128)(2,1)S(1)}, bf16[384,512]{1,0:T(8,128)(2,1)S(1)}, u32[]{:S(2)}, u32[]{:S(2)}) collective-permute-start(bf16[384,512]{1,0:T(8,128)(2,1)S(1)} %constant_dynamic-update-slice_fusion.refs_1_), channel_id=1, source_target_pairs={{0,24},{8,16},{16,8},{24,0},{1,25},{9,17},{17,9},{25,1},{2,26},{10... | collective-permute-start | bytes 1179656 | tf_op jit(solution)/shard_map/ppermute | solution.py:24
  45.3 0.0 collective-permute-done.11
  45.3 1.4 %collective-permute-start.4 = (bf16[384,512]{1,0:T(8,128)(2,1)S(1)}, bf16[384,512]{1,0:T(8,128)(2,1)S(1)}, u32[]{:S(2)}, u32[]{:S(2)}) collective-permute-start(bf16[384,512]{1,0:T(8,128)(2,1)S(1)} %constant_dynamic-update-slice_fusion.refs_1_), channel_id=1, source_target_pairs={{0,16},{8,24},{16,0},{24,8},{1,17},{9,25},{17,1},{25,9},{2,18},{10... | collective-permute-start | bytes 1179656 | tf_op jit(solution)/shard_map/ppermute | solution.py:24
  46.7 0.0 collective-permute-done.9
  46.7 0.6 collective-permute-start.3
  47.4 0.6 pad_add_fusion.where_ref
  48.0 0.0 collective-permute-done.10
  48.0 1.5 %collective-permute-start.7 = (bf16[512,128]{1,0:T(8,128)(2,1)}, bf16[512,128]{1,0:T(8,128)(2,1)S(1)}, u32[]{:S(2)}, u32[]{:S(2)}) collective-permute-start(bf16[512,128]{1,0:T(8,128)(2,1)} %shard_map.73.refs_5_), channel_id=1, source_target_pairs={{0,4},{2,6},{1,5},{3,7},{8,12},{10,14},{9,13},{11,15},{16,20},{18,... | collective-permute-start | bytes 393224 | tf_op jit(solution)/shard_map/ppermute | solution.py:195
  49.5 0.0 collective-permute-done.8.refs_8_
  49.5 0.0 copy-start.9
  49.6 2.2 %collective-permute-start.6 = (bf16[512,128]{1,0:T(8,128)(2,1)}, bf16[512,128]{1,0:T(8,128)(2,1)S(1)}, u32[]{:S(2)}, u32[]{:S(2)}) collective-permute-start(bf16[512,128]{1,0:T(8,128)(2,1)} %shard_map.73.refs_5_), channel_id=1, source_target_pairs={{0,2},{2,4},{4,6},{1,3},{3,5},{5,7},{8,10},{10,12},{12,14},{9,11},... | collective-permute-start | bytes 393224 | tf_op jit(solution)/shard_map/ppermute | solution.py:195
  51.8 0.0 copy-start.1
  51.9 0.5 collective-permute-done.7.refs_7_
  52.4 0.0 copy-start.10
  52.4 1.5 %collective-permute-start.14 = (bf16[384,512]{1,0:T(8,128)(2,1)S(1)}, bf16[384,512]{1,0:T(8,128)(2,1)S(1)}, u32[]{:S(2)}, u32[]{:S(2)}) collective-permute-start(bf16[384,512]{1,0:T(8,128)(2,1)S(1)} %constant_dynamic-update-slice_fusion.3.refs_1_), channel_id=1, source_target_pairs={{0,24},{8,16},{16,8},{24,0},{1,25},{9,17},{17,9},{25,1},{2,26},{10... | collective-permute-start | bytes 1179656 | tf_op jit(solution)/shard_map/ppermute | solution.py:24
  53.8 0.8 collective-permute-done.6.refs_6_
  54.6 0.0 copy-start.11
  54.6 1.4 %collective-permute-start.13 = (bf16[384,512]{1,0:T(8,128)(2,1)S(1)}, bf16[384,512]{1,0:T(8,128)(2,1)S(1)}, u32[]{:S(2)}, u32[]{:S(2)}) collective-permute-start(bf16[384,512]{1,0:T(8,128)(2,1)S(1)} %constant_dynamic-update-slice_fusion.3.refs_1_), channel_id=1, source_target_pairs={{0,16},{8,24},{16,0},{24,8},{1,17},{9,25},{17,1},{25,9},{2,18},{10... | collective-permute-start | bytes 1179656 | tf_op jit(solution)/shard_map/ppermute | solution.py:24
  56.0 0.9 collective-permute-done.5.refs_4_
  56.9 0.0 copy-start.6
  56.9 1.4 %collective-permute-start.12 = (bf16[384,512]{1,0:T(8,128)(2,1)S(1)}, bf16[384,512]{1,0:T(8,128)(2,1)S(1)}, u32[]{:S(2)}, u32[]{:S(2)}) collective-permute-start(bf16[384,512]{1,0:T(8,128)(2,1)S(1)} %constant_dynamic-update-slice_fusion.3.refs_1_), channel_id=1, source_target_pairs={{0,8},{8,0},{16,24},{24,16},{1,9},{9,1},{17,25},{25,17},{2,10},{10... | collective-permute-start | bytes 1179656 | tf_op jit(solution)/shard_map/ppermute | solution.py:24
  58.2 7.4 %collective-permute-done.4.refs_3_ = bf16[384,512]{1,0:T(8,128)(2,1)S(1)} collective-permute-done((bf16[384,512]{1,0:T(8,128)(2,1)S(1)}, bf16[384,512]{1,0:T(8,128)(2,1)S(1)}, u32[]{:S(2)}, u32[]{:S(2)}) %collective-permute-start.4) | collective-permute-done | bytes 393248 | tf_op jit(solution)/shard_map/ppermute | solution.py:24
  65.7 0.0 copy-start.7
  65.7 0.0 collective-permute-done.3.refs_2_
  65.7 0.0 copy-done.5
  65.7 0.0 copy-done.9
  65.7 0.0 copy-done.10
  65.7 0.0 copy-done.11
  65.7 0.0 copy-done.6
  65.7 0.7 copy-done.7
  66.4 0.8 copy-done.8
  67.2 14.6 %shard_map.74.att_ref = bf16[512,512]{1,0:T(8,128)(2,1)} custom-call(s32[3]{0:T(128)} %pad_add_fusion.where_ref, s32[8,16]{1,0:T(8,128)} %chosen_ref.1, bf16[512,2048]{1,0:T(8,128)(2,1)} %tok_ref.3, bf16[512,512]{1,0:T(8,128)(2,1)} %refs_0_.2, bf16[384,512]{1,0:T(8,128)(2,1)} %copy-done.5, bf16[384,512]{1,0:T(8,128)(2,1)} %copy-done.8, ...), custom_call_target="tpu_custom_call" | custom-call | flops 34359738368 | bytes 2097152 | tf_op jit(solution)/shard_map/pallas_call | solution.py:201
  81.8 0.0 copy-done.1
  81.8 0.0 collective-permute-done.14.refs_4_
  81.8 0.0 copy-start.2
  81.8 0.0 collective-permute-done.13.refs_3_
  81.9 0.0 copy-start.3
  81.9 0.0 collective-permute-done.12.refs_2_
  81.9 0.7 copy-done.2
  82.6 0.2 copy-done.3
  82.7 0.7 copy-done.4
  83.5 4.1 %shard_map.75 = (bf16[256,2048]{1,0:T(8,128)(2,1)}, bf16[256,2048]{1,0:T(8,128)(2,1)}) custom-call(s32[3]{0:T(128)} %pad_add_fusion.where_ref, bf16[512,512]{1,0:T(8,128)(2,1)} %shard_map.74.att_ref, bf16[512,512]{1,0:T(8,128)(2,1)} %refs_0_.3, bf16[384,512]{1,0:T(8,128)(2,1)} %copy-done.1, bf16[384,512]{1,0:T(8,128)(2,1)} %copy-done.4, ...), custom_call_target="tpu_custom_call" | custom-call | tf_op jit(solution)/shard_map/pallas_call | solution.py:228
  87.5 0.0 collective-permute-start.15
  87.5 2.9 %collective-permute-done.15.b_ref = bf16[256,2048]{1,0:T(8,128)(2,1)S(1)} collective-permute-done((bf16[256,2048]{1,0:T(8,128)(2,1)}, bf16[256,2048]{1,0:T(8,128)(2,1)S(1)}, u32[]{:S(2)}, u32[]{:S(2)}) %collective-permute-start.15) | collective-permute-done | bytes 1048608 | tf_op jit(solution)/shard_map/ppermute | solution.py:24
  90.4 1.0 %copy-done = bf16[256,2048]{1,0:T(8,128)(2,1)} copy-done((bf16[256,2048]{1,0:T(8,128)(2,1)}, bf16[256,2048]{1,0:T(8,128)(2,1)S(1)}, u32[]{:S(2)}) %copy-start) | copy-done | bytes 1048600
  91.4 3.2 %shard_map.76 = bf16[256,2048]{1,0:T(8,128)(2,1)} custom-call(bf16[256,2048]{1,0:T(8,128)(2,1)} %get-tuple-element.11.a_ref, bf16[256,2048]{1,0:T(8,128)(2,1)} %copy-done, f32[1,2048]{1,0:T(1,128)} %bitcast.8), custom_call_target="tpu_custom_call" | custom-call | tf_op jit(solution)/shard_map/pallas_call | solution.py:240
  (10 shorter events, 0.1 us)
Async XLA Ops:
  15.7 28.0 %collective-permute-start.2 = (bf16[128,512]{1,0:T(8,128)(2,1)S(1)}, bf16[128,512]{1,0:T(8,128)(2,1)S(1)}, u32[]{:S(2)}, u32[]{:S(2)}) collective-permute-start(bf16[128,512]{1,0:T(8,128)(2,1)S(1)} %constant_dynamic-slice_fusion.3), channel_id=1, source_target_pairs={{0,6},{2,0},{4,2},{6,4},{1,7},{3,1},{5,3},{7,5},{8,14},{10,8},{12,... | collective-permute-start | bytes 393224 | tf_op jit(solution)/shard_map/ppermute | solution.py:20
  18.2 20.1 %collective-permute-start.1 = (bf16[128,512]{1,0:T(8,128)(2,1)S(1)}, bf16[128,512]{1,0:T(8,128)(2,1)S(1)}, u32[]{:S(2)}, u32[]{:S(2)}) collective-permute-start(bf16[128,512]{1,0:T(8,128)(2,1)S(1)} %constant_dynamic-slice_fusion.3), channel_id=1, source_target_pairs={{0,4},{2,6},{4,0},{6,2},{1,5},{3,7},{5,1},{7,3},{8,12},{10,14},{12... | collective-permute-start | bytes 393224 | tf_op jit(solution)/shard_map/ppermute | solution.py:20
  19.1 18.9 %collective-permute-start = (bf16[128,512]{1,0:T(8,128)(2,1)S(1)}, bf16[128,512]{1,0:T(8,128)(2,1)S(1)}, u32[]{:S(2)}, u32[]{:S(2)}) collective-permute-start(bf16[128,512]{1,0:T(8,128)(2,1)S(1)} %constant_dynamic-slice_fusion.3), channel_id=1, source_target_pairs={{0,2},{2,4},{4,6},{6,0},{1,3},{3,5},{5,7},{7,1},{8,10},{10,12},{12... | collective-permute-start | bytes 393224 | tf_op jit(solution)/shard_map/ppermute | solution.py:20
  20.0 25.3 %collective-permute-start.11 = (bf16[128,512]{1,0:T(8,128)(2,1)S(1)}, bf16[128,512]{1,0:T(8,128)(2,1)S(1)}, u32[]{:S(2)}, u32[]{:S(2)}) collective-permute-start(bf16[128,512]{1,0:T(8,128)(2,1)S(1)} %constant_dynamic-slice_fusion), channel_id=1, source_target_pairs={{0,6},{2,0},{4,2},{6,4},{1,7},{3,1},{5,3},{7,5},{8,14},{10,8},{12,... | collective-permute-start | bytes 393224 | tf_op jit(solution)/shard_map/ppermute | solution.py:20
  23.9 24.1 %collective-permute-start.10 = (bf16[128,512]{1,0:T(8,128)(2,1)S(1)}, bf16[128,512]{1,0:T(8,128)(2,1)S(1)}, u32[]{:S(2)}, u32[]{:S(2)}) collective-permute-start(bf16[128,512]{1,0:T(8,128)(2,1)S(1)} %constant_dynamic-slice_fusion), channel_id=1, source_target_pairs={{0,4},{2,6},{4,0},{6,2},{1,5},{3,7},{5,1},{7,3},{8,12},{10,14},{12... | collective-permute-start | bytes 393224 | tf_op jit(solution)/shard_map/ppermute | solution.py:20
  38.0 8.8 %collective-permute-start.9 = (bf16[128,512]{1,0:T(8,128)(2,1)S(1)}, bf16[128,512]{1,0:T(8,128)(2,1)S(1)}, u32[]{:S(2)}, u32[]{:S(2)}) collective-permute-start(bf16[128,512]{1,0:T(8,128)(2,1)S(1)} %constant_dynamic-slice_fusion), channel_id=1, source_target_pairs={{0,2},{2,4},{4,6},{6,0},{1,3},{3,5},{5,7},{7,1},{8,10},{10,12},{12... | collective-permute-start | bytes 393224 | tf_op jit(solution)/shard_map/ppermute | solution.py:20
  38.4 11.2 %collective-permute-start.8 = (bf16[512,128]{1,0:T(8,128)(2,1)}, bf16[512,128]{1,0:T(8,128)(2,1)S(1)}, u32[]{:S(2)}, u32[]{:S(2)}) collective-permute-start(bf16[512,128]{1,0:T(8,128)(2,1)} %shard_map.73.refs_5_), channel_id=1, source_target_pairs={{0,6},{1,7},{8,14},{9,15},{16,22},{17,23},{24,30},{25,31}} | collective-permute-start | bytes 393224 | tf_op jit(solution)/shard_map/ppermute | solution.py:195
  43.8 21.9 %copy-start.5 = (bf16[384,512]{1,0:T(8,128)(2,1)}, bf16[384,512]{1,0:T(8,128)(2,1)S(1)}, u32[]{:S(2)}) copy-start(bf16[384,512]{1,0:T(8,128)(2,1)S(1)} %constant_dynamic-update-slice_fusion.refs_1_) | copy-start | bytes 1179652
  43.8 13.1 %collective-permute-start.5 = (bf16[384,512]{1,0:T(8,128)(2,1)S(1)}, bf16[384,512]{1,0:T(8,128)(2,1)S(1)}, u32[]{:S(2)}, u32[]{:S(2)}) collective-permute-start(bf16[384,512]{1,0:T(8,128)(2,1)S(1)} %constant_dynamic-update-slice_fusion.refs_1_), channel_id=1, source_target_pairs={{0,24},{8,16},{16,8},{24,0},{1,25},{9,17},{17,9},{25,1},{2,26},{10... | collective-permute-start | bytes 1179656 | tf_op jit(solution)/shard_map/ppermute | solution.py:24
  45.3 20.4 %collective-permute-start.4 = (bf16[384,512]{1,0:T(8,128)(2,1)S(1)}, bf16[384,512]{1,0:T(8,128)(2,1)S(1)}, u32[]{:S(2)}, u32[]{:S(2)}) collective-permute-start(bf16[384,512]{1,0:T(8,128)(2,1)S(1)} %constant_dynamic-update-slice_fusion.refs_1_), channel_id=1, source_target_pairs={{0,16},{8,24},{16,0},{24,8},{1,17},{9,25},{17,1},{25,9},{2,18},{10... | collective-permute-start | bytes 1179656 | tf_op jit(solution)/shard_map/ppermute | solution.py:24
  46.7 19.0 %collective-permute-start.3 = (bf16[384,512]{1,0:T(8,128)(2,1)S(1)}, bf16[384,512]{1,0:T(8,128)(2,1)S(1)}, u32[]{:S(2)}, u32[]{:S(2)}) collective-permute-start(bf16[384,512]{1,0:T(8,128)(2,1)S(1)} %constant_dynamic-update-slice_fusion.refs_1_), channel_id=1, source_target_pairs={{0,8},{8,0},{16,24},{24,16},{1,9},{9,1},{17,25},{25,17},{2,10},{10... | collective-permute-start | bytes 1179656 | tf_op jit(solution)/shard_map/ppermute | solution.py:24
  48.0 4.4 %collective-permute-start.7 = (bf16[512,128]{1,0:T(8,128)(2,1)}, bf16[512,128]{1,0:T(8,128)(2,1)S(1)}, u32[]{:S(2)}, u32[]{:S(2)}) collective-permute-start(bf16[512,128]{1,0:T(8,128)(2,1)} %shard_map.73.refs_5_), channel_id=1, source_target_pairs={{0,4},{2,6},{1,5},{3,7},{8,12},{10,14},{9,13},{11,15},{16,20},{18,... | collective-permute-start | bytes 393224 | tf_op jit(solution)/shard_map/ppermute | solution.py:195
  49.5 16.2 %copy-start.9 = (bf16[512,128]{1,0:T(8,128)(2,1)}, bf16[512,128]{1,0:T(8,128)(2,1)S(1)}, u32[]{:S(2)}) copy-start(bf16[512,128]{1,0:T(8,128)(2,1)S(1)} %collective-permute-done.8.refs_8_) | copy-start | bytes 393220
  49.6 5.1 %collective-permute-start.6 = (bf16[512,128]{1,0:T(8,128)(2,1)}, bf16[512,128]{1,0:T(8,128)(2,1)S(1)}, u32[]{:S(2)}, u32[]{:S(2)}) collective-permute-start(bf16[512,128]{1,0:T(8,128)(2,1)} %shard_map.73.refs_5_), channel_id=1, source_target_pairs={{0,2},{2,4},{4,6},{1,3},{3,5},{5,7},{8,10},{10,12},{12,14},{9,11},... | collective-permute-start | bytes 393224 | tf_op jit(solution)/shard_map/ppermute | solution.py:195
  51.8 30.0 %copy-start.1 = (bf16[384,512]{1,0:T(8,128)(2,1)}, bf16[384,512]{1,0:T(8,128)(2,1)S(1)}, u32[]{:S(2)}) copy-start(bf16[384,512]{1,0:T(8,128)(2,1)S(1)} %constant_dynamic-update-slice_fusion.3.refs_1_) | copy-start | bytes 1179652
  52.4 13.4 %copy-start.10 = (bf16[512,128]{1,0:T(8,128)(2,1)}, bf16[512,128]{1,0:T(8,128)(2,1)S(1)}, u32[]{:S(2)}) copy-start(bf16[512,128]{1,0:T(8,128)(2,1)S(1)} %collective-permute-done.7.refs_7_) | copy-start | bytes 393220
  52.4 29.5 %collective-permute-start.14 = (bf16[384,512]{1,0:T(8,128)(2,1)S(1)}, bf16[384,512]{1,0:T(8,128)(2,1)S(1)}, u32[]{:S(2)}, u32[]{:S(2)}) collective-permute-start(bf16[384,512]{1,0:T(8,128)(2,1)S(1)} %constant_dynamic-update-slice_fusion.3.refs_1_), channel_id=1, source_target_pairs={{0,24},{8,16},{16,8},{24,0},{1,25},{9,17},{17,9},{25,1},{2,26},{10... | collective-permute-start | bytes 1179656 | tf_op jit(solution)/shard_map/ppermute | solution.py:24
  54.6 11.1 %copy-start.11 = (bf16[512,128]{1,0:T(8,128)(2,1)}, bf16[512,128]{1,0:T(8,128)(2,1)S(1)}, u32[]{:S(2)}) copy-start(bf16[512,128]{1,0:T(8,128)(2,1)S(1)} %collective-permute-done.6.refs_6_) | copy-start | bytes 393220
  54.6 27.2 %collective-permute-start.13 = (bf16[384,512]{1,0:T(8,128)(2,1)S(1)}, bf16[384,512]{1,0:T(8,128)(2,1)S(1)}, u32[]{:S(2)}, u32[]{:S(2)}) collective-permute-start(bf16[384,512]{1,0:T(8,128)(2,1)S(1)} %constant_dynamic-update-slice_fusion.3.refs_1_), channel_id=1, source_target_pairs={{0,16},{8,24},{16,0},{24,8},{1,17},{9,25},{17,1},{25,9},{2,18},{10... | collective-permute-start | bytes 1179656 | tf_op jit(solution)/shard_map/ppermute | solution.py:24
  56.9 8.9 %copy-start.6 = (bf16[384,512]{1,0:T(8,128)(2,1)}, bf16[384,512]{1,0:T(8,128)(2,1)S(1)}, u32[]{:S(2)}) copy-start(bf16[384,512]{1,0:T(8,128)(2,1)S(1)} %collective-permute-done.5.refs_4_) | copy-start | bytes 1179652
  56.9 25.0 %collective-permute-start.12 = (bf16[384,512]{1,0:T(8,128)(2,1)S(1)}, bf16[384,512]{1,0:T(8,128)(2,1)S(1)}, u32[]{:S(2)}, u32[]{:S(2)}) collective-permute-start(bf16[384,512]{1,0:T(8,128)(2,1)S(1)} %constant_dynamic-update-slice_fusion.3.refs_1_), channel_id=1, source_target_pairs={{0,8},{8,0},{16,24},{24,16},{1,9},{9,1},{17,25},{25,17},{2,10},{10... | collective-permute-start | bytes 1179656 | tf_op jit(solution)/shard_map/ppermute | solution.py:24
  65.7 0.8 copy-start.7
  66.4 0.8 copy-start.8
  81.8 0.7 copy-start.2
  81.9 0.9 copy-start.3
  82.7 0.7 copy-start.4
  87.5 2.9 %collective-permute-start.15 = (bf16[256,2048]{1,0:T(8,128)(2,1)}, bf16[256,2048]{1,0:T(8,128)(2,1)S(1)}, u32[]{:S(2)}, u32[]{:S(2)}) collective-permute-start(bf16[256,2048]{1,0:T(8,128)(2,1)} %get-tuple-element.12), channel_id=1, source_target_pairs={{0,1},{1,0},{2,3},{3,2},{4,5},{5,4},{6,7},{7,6},{8,9},{9,8},{10,11... | collective-permute-start | bytes 3145736 | tf_op jit(solution)/shard_map/ppermute | solution.py:24
  90.4 1.0 %copy-start = (bf16[256,2048]{1,0:T(8,128)(2,1)}, bf16[256,2048]{1,0:T(8,128)(2,1)S(1)}, u32[]{:S(2)}) copy-start(bf16[256,2048]{1,0:T(8,128)(2,1)S(1)} %collective-permute-done.15.b_ref) | copy-start | bytes 3145732

commit v3 on v2

--- a/solution.py
+++ b/solution.py
@@ -124,7 +124,7 @@
         ).astype(BF16)
         return carry
 
-    lax.fori_loop(0, blocks, one_block, 0)
+    lax.fori_loop(0, blocks, one_block, 0, unroll=2)
 
 
 def project_kernel(where_ref, att_ref, *refs, n_weights, kv_count):
@@ -167,35 +167,42 @@
         and out_weight.shape[1] % 128 == 0
     )
     if direct:
-        pair_piece = jnp.concatenate(
-            [piece_of(key_matrix, dp_count), piece_of(value_matrix, dp_count)], axis=1
-        )
-        pair_line = lax.all_gather(pair_piece, "kv", axis=0)
-        q_piece, pair_line = lax.optimization_barrier((piece_of(query_weight, dp_count), pair_line))
-        q_got = along_kv(q_piece, kv_count)
-        pair_whole = lax.all_gather(pair_line, "dp", axis=0)
+        columns = query_weight.shape[1]
+        both = jnp.concatenate(
+            [
+                piece_of(query_weight, dp_count),
+                piece_of(key_matrix, dp_count),
+                piece_of(value_matrix, dp_count),
+            ],
+            axis=1,
+        )
+        got = along_kv(both, kv_count)
+        pair_shard = jnp.concatenate([key_matrix, value_matrix], axis=1)
+        pair_parts = across_dp(pair_shard, [g[:, columns:] for g in got], dp_count)
+        q_parts = across_dp(query_weight, [g[:, :columns] for g in got], dp_count)
+        o_got = along_kv(piece_of(out_weight, dp_count), kv_count)
+        o_parts = across_dp(out_weight, o_got, dp_count)
     else:
         pair_shard = jnp.concatenate([key_matrix, value_matrix], axis=1)
-        pair_whole = lax.all_gather(pair_shard, "kv", axis=0)[None]
+        pair_parts = [lax.all_gather(pair_shard, "kv", axis=0, tiled=True)]
         q_parts = [lax.all_gather(query_weight, "kv", axis=0, tiled=True)]
         o_parts = [lax.all_gather(out_weight, "kv", axis=1, tiled=True)]
     vmem = pl.BlockSpec(memory_space=pltpu.VMEM)
     smem = pl.BlockSpec(memory_space=pltpu.SMEM)
-    pair_width = pair_whole.shape[-1]
+    pair_width = pair_shard.shape[1]
     pairs = pl.pallas_call(
-        pair_project,
+        functools.partial(pair_project, kv_count=kv_count),
         out_shape=jax.ShapeDtypeStruct((tok_rows, pair_width), BF16),
-        in_specs=[vmem, vmem],
+        in_specs=[smem, vmem] + [vmem] * len(pair_parts),
         out_specs=vmem,
-        scratch_shapes=[pltpu.VMEM((model, pair_width), BF16)],
-    )(tokens, pair_whole)
+        scratch_shapes=[
+            pltpu.VMEM((kv_count, shard, pair_width) if direct else (1, model, pair_width), BF16)
+        ],
+    )(where, tokens, *pair_parts)
     if direct:
         row_parts = [pairs]
         for s in range(1, kv_count):
             row_parts.append(lax.ppermute(pairs, "kv", [(i, i + s) for i in range(kv_count - s)]))
-        q_parts = across_dp(query_weight, q_got, dp_count)
-        o_got = along_kv(piece_of(out_weight, dp_count), kv_count)
-        o_parts = across_dp(out_weight, o_got, dp_count)
     else:
         row_parts = [lax.all_gather(pairs, "kv", axis=0, tiled=True)]
     attended = pl.pallas_call(
@@ -245,13 +252,11 @@
     )(mine, theirs, out_gain.reshape(1, -1))
 
 
-def pair_project(tok_ref, w_ref, out_ref, w_full):
-    dp_count, kv_count, rows = w_ref.shape[:3]
-    for k in range(kv_count):
-        for d in range(dp_count):
-            at = (k * dp_count + d) * rows
-            w_full[at:at + rows] = w_ref[d, k]
-    out_ref[...] = jnp.dot(tok_ref[...], w_full[...], preferred_element_type=F32).astype(BF16)
+def pair_project(where_ref, tok_ref, *refs, kv_count):
+    *w_refs, out_ref, w_full = refs
+    place(w_refs, w_full, where_ref[0], where_ref[1], kv_count)
+    whole = w_full[...].reshape(-1, w_full.shape[-1])
+    out_ref[...] = jnp.dot(tok_ref[...], whole, preferred_element_type=F32).astype(BF16)
 
 
 def solution(mesh):

time: 95 us -> 89.9 us (0.946)
  blocking collectives: 24.7 us -> 0 us
  waiting for transfers between devices: 12.5 us -> 25 us
  starting transfers between devices: 24.8 us -> 31.5 us
  Pallas kernels: 25 us -> 23.4 us
  local copies, waits for them, and re-layouts: 6.79 us -> 7.87 us
  other arithmetic: 0.6 us -> 1.55 us
    all_gather x2 -> x0, blocking collectives: 24.7 us -> none  [the longest x1 13.9 us: layer(): pair_line = lax.all_gather(pair_piece, 'kv', axis=0)]
    ppermute x6, waiting for transfers between devices: 0.02 us -> 14 us  [shift(): return lax.ppermute(x, axis, [(i, (i + by) % count) for i in range(count)])]
    ppermute x7 -> x10, starting transfers between devices: 7.78 us -> 12.9 us  [swap(): return lax.ppermute(x, axis, [(i, i ^ bit) for i in range(count)])]
    ppermute x6, starting transfers between devices: 7.87 us -> 10.8 us  [shift(): return lax.ppermute(x, axis, [(i, (i + by) % count) for i in range(count)])]
    unnamed x28 -> x36, local copies, waits for them, and re-layouts: 4.08 us -> 5.97 us
    ppermute x7 -> x10, waiting for transfers between devices: 11.2 us -> 9.46 us  [swap(): return lax.ppermute(x, axis, [(i, i ^ bit) for i in range(count)])]
    pallas_call x1, Pallas kernels: 14.6 us -> 13 us  [layer(): pl.pallas_call(functools.partial(attend_kernel, n_weights=len(q_parts), n...]
    ppermute x3, starting transfers between devices: 9.14 us -> 7.78 us  [layer(): lax.ppermute(pairs, 'kv', [(i, i + s) for i in range(kv_count - s)])]
  transfers between devices with their start and end apart: 16 -> 19, of which waited for: 5 -> 6; matrix products, arithmetic and copies ran while one was open for 2% -> 3% of each run, Pallas kernels for 19% -> 18%
where the time goes in v3:
time: 89.9 us; the launch traced here: 89.5 us
  starting transfers between devices  31.5 us (35%)
  waiting for transfers between devices  25 us (28%)
  Pallas kernels  23.4 us (26%)
  local copies, waits for them, and re-layouts  7.87 us (9%)
  other arithmetic  1.55 us (2%)
    ppermute x6, waiting for transfers between devices, shift(): return lax.ppermute(x, axis, [(i, (i + by) % count) for i in range(count)])  14 us
    pallas_call x1, Pallas kernels, layer(): pl.pallas_call(functools.partial(attend_kernel, n_weights=len(q_parts), n...  13 us
    ppermute x10, starting transfers between devices, swap(): return lax.ppermute(x, axis, [(i, i ^ bit) for i in range(count)])  12.9 us
    ppermute x6, starting transfers between devices, shift(): return lax.ppermute(x, axis, [(i, (i + by) % count) for i in range(count)])  10.8 us
    ppermute x10, waiting for transfers between devices, swap(): return lax.ppermute(x, axis, [(i, i ^ bit) for i in range(count)])  9.46 us
    ppermute x3, starting transfers between devices, layer(): lax.ppermute(pairs, 'kv', [(i, i + s) for i in range(kv_count - s)])  7.78 us
    unnamed x36, local copies, waits for them, and re-layouts  5.97 us
    pallas_call x1, Pallas kernels, layer(): pl.pallas_call(functools.partial(project_kernel, n_weights=len(o_parts),...  4.05 us
  transfers between devices with their start and end apart: 19, of which 6 were waited for; matrix products, arithmetic and copies ran while one was open for 3% of the time, Pallas kernels for 18%

profile of v3, /device:TPU:0, one launch (start us, length us, event | category | flops | bytes accessed | tf_op | source)
XLA Modules:
  0.0 89.5 jit_solution(14366108028374817354)
XLA Ops:
  0.0 1.0 %copy.8 = bf16[512,64]{1,0:T(8,128)(2,1)S(1)} copy(bf16[512,64]{0,1:T(8,128)(2,1)} %param.10) | data formatting | bytes 131072 | tf_op args[3]
  1.0 1.0 %copy.9 = bf16[512,64]{1,0:T(8,128)(2,1)S(1)} copy(bf16[512,64]{0,1:T(8,128)(2,1)} %param.11) | data formatting | bytes 131072 | tf_op args[4]
  1.9 0.9 %constant_dynamic-slice_fusion.3 = bf16[128,512]{1,0:T(8,128)(2,1)S(1)} fusion(bf16[512,512]{1,0:T(8,128)(2,1)} %refs_0_.2, s32[]{:T(128)S(6)} %select_n.2), kind=kLoop, calls=%fused_computation.10 | loop fusion | bytes 262148 | tf_op jit(solution)/shard_map/dynamic_slice | solution.py:29
  2.9 0.1 pad_maximum_fusion.1
  3.0 5.1 %collective-permute-start.2 = (bf16[128,640]{1,0:T(8,128)(2,1)S(1)}, bf16[128,640]{1,0:T(8,128)(2,1)S(1)}, u32[]{:S(2)}, u32[]{:S(2)}) collective-permute-start(bf16[128,640]{1,0:T(8,128)(2,1)S(1)} %pad_maximum_fusion.1), channel_id=1, source_target_pairs={{0,6},{2,0},{4,2},{6,4},{1,7},{3,1},{5,3},{7,5},{8,14},{10,8},{12,... | collective-permute-start | bytes 491528 | tf_op jit(solution)/shard_map/ppermute | solution.py:20
  8.1 0.0 collective-permute-start.1
  8.1 1.0 %collective-permute-start = (bf16[128,640]{1,0:T(8,128)(2,1)S(1)}, bf16[128,640]{1,0:T(8,128)(2,1)S(1)}, u32[]{:S(2)}, u32[]{:S(2)}) collective-permute-start(bf16[128,640]{1,0:T(8,128)(2,1)S(1)} %pad_maximum_fusion.1), channel_id=1, source_target_pairs={{0,2},{2,4},{4,6},{6,0},{1,3},{3,5},{5,7},{7,1},{8,10},{10,12},{12... | collective-permute-start | bytes 491528 | tf_op jit(solution)/shard_map/ppermute | solution.py:20
  9.1 0.9 %constant_dynamic-slice_fusion = bf16[128,512]{1,0:T(8,128)(2,1)S(1)} fusion(bf16[512,512]{1,0:T(8,128)(2,1)} %refs_0_.3, s32[]{:T(128)S(6)} %select_n.2), kind=kLoop, calls=%fused_computation.7 | loop fusion | bytes 262148 | tf_op jit(solution)/shard_map/dynamic_slice | solution.py:29
  10.0 2.9 %collective-permute-start.14 = (bf16[128,512]{1,0:T(8,128)(2,1)S(1)}, bf16[128,512]{1,0:T(8,128)(2,1)S(1)}, u32[]{:S(2)}, u32[]{:S(2)}) collective-permute-start(bf16[128,512]{1,0:T(8,128)(2,1)S(1)} %constant_dynamic-slice_fusion), channel_id=1, source_target_pairs={{0,6},{2,0},{4,2},{6,4},{1,7},{3,1},{5,3},{7,5},{8,14},{10,8},{12,... | collective-permute-start | bytes 393224 | tf_op jit(solution)/shard_map/ppermute | solution.py:20
  12.9 0.0 collective-permute-start.12
  12.9 0.8 pad_maximum_fusion.2.refs_0_
  13.7 0.0 collective-permute-done.2
  13.7 11.6 %collective-permute-done.1 = bf16[128,640]{1,0:T(8,128)(2,1)S(1)} collective-permute-done((bf16[128,640]{1,0:T(8,128)(2,1)S(1)}, bf16[128,640]{1,0:T(8,128)(2,1)S(1)}, u32[]{:S(2)}, u32[]{:S(2)}) %collective-permute-start.1) | collective-permute-done | bytes 163872 | tf_op jit(solution)/shard_map/ppermute | solution.py:20
  25.3 0.0 collective-permute-done
  25.3 0.0 copy-start.2
  25.3 2.5 %collective-permute-start.8 = (bf16[384,128]{1,0:T(8,128)(2,1)S(1)}, bf16[384,128]{1,0:T(8,128)(2,1)S(1)}, u32[]{:S(2)}, u32[]{:S(2)}) collective-permute-start(bf16[384,128]{1,0:T(8,128)(2,1)S(1)} %pad_maximum_fusion.3.refs_1_), channel_id=1, source_target_pairs={{0,24},{8,16},{16,8},{24,0},{1,25},{9,17},{17,9},{25,1},{2,26},{10... | collective-permute-start | bytes 294920 | tf_op jit(solution)/shard_map/ppermute | solution.py:24
  27.8 0.5 collective-permute-start.7
  28.3 0.5 collective-permute-start.6
  29.0 0.0 copy-start.3
  29.0 3.1 %collective-permute-done.8.refs_4_ = bf16[384,128]{1,0:T(8,128)(2,1)S(1)} collective-permute-done((bf16[384,128]{1,0:T(8,128)(2,1)S(1)}, bf16[384,128]{1,0:T(8,128)(2,1)S(1)}, u32[]{:S(2)}, u32[]{:S(2)}) %collective-permute-start.8) | collective-permute-done | bytes 98336 | tf_op jit(solution)/shard_map/ppermute | solution.py:24
  32.0 2.4 %collective-permute-start.5 = (bf16[384,512]{1,0:T(8,128)(2,1)S(1)}, bf16[384,512]{1,0:T(8,128)(2,1)S(1)}, u32[]{:S(2)}, u32[]{:S(2)}) collective-permute-start(bf16[384,512]{1,0:T(8,128)(2,1)S(1)} %pad_maximum_fusion.refs_1_), channel_id=1, source_target_pairs={{0,24},{8,16},{16,8},{24,0},{1,25},{9,17},{17,9},{25,1},{2,26},{10... | collective-permute-start | bytes 1179656 | tf_op jit(solution)/shard_map/ppermute | solution.py:24
  34.4 3.5 %collective-permute-done.7.refs_3_ = bf16[384,128]{1,0:T(8,128)(2,1)S(1)} collective-permute-done((bf16[384,128]{1,0:T(8,128)(2,1)S(1)}, bf16[384,128]{1,0:T(8,128)(2,1)S(1)}, u32[]{:S(2)}, u32[]{:S(2)}) %collective-permute-start.7) | collective-permute-done | bytes 98336 | tf_op jit(solution)/shard_map/ppermute | solution.py:24
  37.9 1.6 %collective-permute-start.4 = (bf16[384,512]{1,0:T(8,128)(2,1)S(1)}, bf16[384,512]{1,0:T(8,128)(2,1)S(1)}, u32[]{:S(2)}, u32[]{:S(2)}) collective-permute-start(bf16[384,512]{1,0:T(8,128)(2,1)S(1)} %pad_maximum_fusion.refs_1_), channel_id=1, source_target_pairs={{0,16},{8,24},{16,0},{24,8},{1,17},{9,25},{17,1},{25,9},{2,18},{10... | collective-permute-start | bytes 1179656 | tf_op jit(solution)/shard_map/ppermute | solution.py:24
  39.5 0.0 collective-permute-done.6.refs_2_
  39.5 0.6 collective-permute-start.3
  40.2 0.7 pad_add_fusion.where_ref
  40.8 0.0 copy-done.2
  40.9 0.0 copy-done.7
  40.9 0.0 copy-done.8
  40.9 0.0 copy-done.9
  40.9 3.1 %shard_map.73.refs_5_ = bf16[512,128]{1,0:T(8,128)(2,1)} custom-call(s32[3]{0:T(128)} %pad_add_fusion.where_ref, bf16[512,2048]{1,0:T(8,128)(2,1)} %tok_ref.3, bf16[512,128]{1,0:T(8,128)(2,1)} %pad_maximum_fusion.2.refs_0_, bf16[384,128]{1,0:T(8,128)(2,1)} %copy-done.2, bf16[384,128]{1,0:T(8,128)(2,1)} %copy-done.9, bf16[384,128]{1,0:T(8,128)(2,1)} %copy-done.8, ...), custom_call_target="tpu_custom_call" | custom-call | tf_op jit(solution)/shard_map/pallas_call | solution.py:193
  44.0 0.0 collective-permute-done.14
  44.0 1.7 %collective-permute-start.13 = (bf16[128,512]{1,0:T(8,128)(2,1)S(1)}, bf16[128,512]{1,0:T(8,128)(2,1)S(1)}, u32[]{:S(2)}, u32[]{:S(2)}) collective-permute-start(bf16[128,512]{1,0:T(8,128)(2,1)S(1)} %constant_dynamic-slice_fusion), channel_id=1, source_target_pairs={{0,4},{2,6},{4,0},{6,2},{1,5},{3,7},{5,1},{7,3},{8,12},{10,14},{12... | collective-permute-start | bytes 393224 | tf_op jit(solution)/shard_map/ppermute | solution.py:20
  45.8 0.0 collective-permute-done.12
  45.8 2.3 %collective-permute-start.11 = (bf16[512,128]{1,0:T(8,128)(2,1)}, bf16[512,128]{1,0:T(8,128)(2,1)S(1)}, u32[]{:S(2)}, u32[]{:S(2)}) collective-permute-start(bf16[512,128]{1,0:T(8,128)(2,1)} %shard_map.73.refs_5_), channel_id=1, source_target_pairs={{0,6},{1,7},{8,14},{9,15},{16,22},{17,23},{24,30},{25,31}} | collective-permute-start | bytes 393224 | tf_op jit(solution)/shard_map/ppermute | solution.py:205
  48.1 2.4 %collective-permute-done.13 = bf16[128,512]{1,0:T(8,128)(2,1)S(1)} collective-permute-done((bf16[128,512]{1,0:T(8,128)(2,1)S(1)}, bf16[128,512]{1,0:T(8,128)(2,1)S(1)}, u32[]{:S(2)}, u32[]{:S(2)}) %collective-permute-start.13) | collective-permute-done | bytes 131104 | tf_op jit(solution)/shard_map/ppermute | solution.py:20
  50.5 4.1 %collective-permute-start.10 = (bf16[512,128]{1,0:T(8,128)(2,1)}, bf16[512,128]{1,0:T(8,128)(2,1)S(1)}, u32[]{:S(2)}, u32[]{:S(2)}) collective-permute-start(bf16[512,128]{1,0:T(8,128)(2,1)} %shard_map.73.refs_5_), channel_id=1, source_target_pairs={{0,4},{2,6},{1,5},{3,7},{8,12},{10,14},{9,13},{11,15},{16,20},{18,... | collective-permute-start | bytes 393224 | tf_op jit(solution)/shard_map/ppermute | solution.py:205
  54.7 0.0 collective-permute-done.11.refs_8_
  54.7 0.0 copy-start.13
  54.7 1.3 %collective-permute-start.9 = (bf16[512,128]{1,0:T(8,128)(2,1)}, bf16[512,128]{1,0:T(8,128)(2,1)S(1)}, u32[]{:S(2)}, u32[]{:S(2)}) collective-permute-start(bf16[512,128]{1,0:T(8,128)(2,1)} %shard_map.73.refs_5_), channel_id=1, source_target_pairs={{0,2},{2,4},{4,6},{1,3},{3,5},{5,7},{8,10},{10,12},{12,14},{9,11},... | collective-permute-start | bytes 393224 | tf_op jit(solution)/shard_map/ppermute | solution.py:205
  56.1 0.0 copy-start.1
  56.1 1.4 %collective-permute-done.10.refs_7_ = bf16[512,128]{1,0:T(8,128)(2,1)S(1)} collective-permute-done((bf16[512,128]{1,0:T(8,128)(2,1)}, bf16[512,128]{1,0:T(8,128)(2,1)S(1)}, u32[]{:S(2)}, u32[]{:S(2)}) %collective-permute-start.10) | collective-permute-done | bytes 131104 | tf_op jit(solution)/shard_map/ppermute | solution.py:205
  57.5 2.8 %collective-permute-start.17 = (bf16[384,512]{1,0:T(8,128)(2,1)S(1)}, bf16[384,512]{1,0:T(8,128)(2,1)S(1)}, u32[]{:S(2)}, u32[]{:S(2)}) collective-permute-start(bf16[384,512]{1,0:T(8,128)(2,1)S(1)} %constant_dynamic-update-slice_fusion.refs_1_), channel_id=1, source_target_pairs={{0,24},{8,16},{16,8},{24,0},{1,25},{9,17},{17,9},{25,1},{2,26},{10... | collective-permute-start | bytes 1179656 | tf_op jit(solution)/shard_map/ppermute | solution.py:24
  60.3 0.0 collective-permute-done.9.refs_6_
  60.3 0.2 collective-permute-start.16
  60.5 0.0 collective-permute-done.5.refs_4_
  60.5 1.7 %collective-permute-start.15 = (bf16[384,512]{1,0:T(8,128)(2,1)S(1)}, bf16[384,512]{1,0:T(8,128)(2,1)S(1)}, u32[]{:S(2)}, u32[]{:S(2)}) collective-permute-start(bf16[384,512]{1,0:T(8,128)(2,1)S(1)} %constant_dynamic-update-slice_fusion.refs_1_), channel_id=1, source_target_pairs={{0,8},{8,0},{16,24},{24,16},{1,9},{9,1},{17,25},{25,17},{2,10},{10... | collective-permute-start | bytes 1179656 | tf_op jit(solution)/shard_map/ppermute | solution.py:24
  62.3 0.0 collective-permute-done.4.refs_3_
  62.3 0.0 collective-permute-done.3.refs_2_
  62.3 0.7 copy-done.11
  63.0 0.7 copy-done.12
  63.8 13.0 %shard_map.74.att_ref = bf16[512,512]{1,0:T(8,128)(2,1)} custom-call(s32[3]{0:T(128)} %pad_add_fusion.where_ref, s32[8,16]{1,0:T(8,128)} %chosen_ref.1, bf16[512,2048]{1,0:T(8,128)(2,1)} %tok_ref.3, bf16[512,512]{1,0:T(8,128)(2,1)} %refs_0_.2, bf16[384,512]{1,0:T(8,128)(2,1)} %copy-done.3, bf16[384,512]{1,0:T(8,128)(2,1)} %copy-done.12, ...), custom_call_target="tpu_custom_call" | custom-call | flops 34359738368 | bytes 2097152 | tf_op jit(solution)/shard_map/pallas_call | solution.py:208
  76.7 0.0 collective-permute-done.17.refs_4_
  76.8 0.0 collective-permute-done.16.refs_3_
  76.8 0.0 copy-start.5
  76.8 0.0 collective-permute-done.15.refs_2_
  76.8 0.7 copy-done.4
  77.5 0.2 copy-done.5
  77.7 0.7 copy-done.6
  78.4 4.0 %shard_map.75 = (bf16[256,2048]{1,0:T(8,128)(2,1)}, bf16[256,2048]{1,0:T(8,128)(2,1)}) custom-call(s32[3]{0:T(128)} %pad_add_fusion.where_ref, bf16[512,512]{1,0:T(8,128)(2,1)} %shard_map.74.att_ref, bf16[512,512]{1,0:T(8,128)(2,1)} %refs_0_.3, bf16[384,512]{1,0:T(8,128)(2,1)} %copy-done.1, bf16[384,512]{1,0:T(8,128)(2,1)} %copy-done.6, ...), custom_call_target="tpu_custom_call" | custom-call | tf_op jit(solution)/shard_map/pallas_call | solution.py:235
  82.4 0.0 collective-permute-start.18
  82.4 2.9 %collective-permute-done.18.b_ref = bf16[256,2048]{1,0:T(8,128)(2,1)S(1)} collective-permute-done((bf16[256,2048]{1,0:T(8,128)(2,1)}, bf16[256,2048]{1,0:T(8,128)(2,1)S(1)}, u32[]{:S(2)}, u32[]{:S(2)}) %collective-permute-start.18) | collective-permute-done | bytes 1048608 | tf_op jit(solution)/shard_map/ppermute | solution.py:24
  85.3 1.0 %copy-done = bf16[256,2048]{1,0:T(8,128)(2,1)} copy-done((bf16[256,2048]{1,0:T(8,128)(2,1)}, bf16[256,2048]{1,0:T(8,128)(2,1)S(1)}, u32[]{:S(2)}) %copy-start) | copy-done | bytes 1048600
  86.3 3.2 %shard_map.76 = bf16[256,2048]{1,0:T(8,128)(2,1)} custom-call(bf16[256,2048]{1,0:T(8,128)(2,1)} %get-tuple-element.7.a_ref, bf16[256,2048]{1,0:T(8,128)(2,1)} %copy-done, f32[1,2048]{1,0:T(1,128)} %bitcast.4), custom_call_target="tpu_custom_call" | custom-call | tf_op jit(solution)/shard_map/pallas_call | solution.py:247
  (29 shorter events, 0.2 us)
Async XLA Ops:
  3.0 10.7 %collective-permute-start.2 = (bf16[128,640]{1,0:T(8,128)(2,1)S(1)}, bf16[128,640]{1,0:T(8,128)(2,1)S(1)}, u32[]{:S(2)}, u32[]{:S(2)}) collective-permute-start(bf16[128,640]{1,0:T(8,128)(2,1)S(1)} %pad_maximum_fusion.1), channel_id=1, source_target_pairs={{0,6},{2,0},{4,2},{6,4},{1,7},{3,1},{5,3},{7,5},{8,14},{10,8},{12,... | collective-permute-start | bytes 491528 | tf_op jit(solution)/shard_map/ppermute | solution.py:20
  8.1 17.2 %collective-permute-start.1 = (bf16[128,640]{1,0:T(8,128)(2,1)S(1)}, bf16[128,640]{1,0:T(8,128)(2,1)S(1)}, u32[]{:S(2)}, u32[]{:S(2)}) collective-permute-start(bf16[128,640]{1,0:T(8,128)(2,1)S(1)} %pad_maximum_fusion.1), channel_id=1, source_target_pairs={{0,4},{2,6},{4,0},{6,2},{1,5},{3,7},{5,1},{7,3},{8,12},{10,14},{12... | collective-permute-start | bytes 491528 | tf_op jit(solution)/shard_map/ppermute | solution.py:20
  8.1 17.2 %collective-permute-start = (bf16[128,640]{1,0:T(8,128)(2,1)S(1)}, bf16[128,640]{1,0:T(8,128)(2,1)S(1)}, u32[]{:S(2)}, u32[]{:S(2)}) collective-permute-start(bf16[128,640]{1,0:T(8,128)(2,1)S(1)} %pad_maximum_fusion.1), channel_id=1, source_target_pairs={{0,2},{2,4},{4,6},{6,0},{1,3},{3,5},{5,7},{7,1},{8,10},{10,12},{12... | collective-permute-start | bytes 491528 | tf_op jit(solution)/shard_map/ppermute | solution.py:20
  10.0 34.0 %collective-permute-start.14 = (bf16[128,512]{1,0:T(8,128)(2,1)S(1)}, bf16[128,512]{1,0:T(8,128)(2,1)S(1)}, u32[]{:S(2)}, u32[]{:S(2)}) collective-permute-start(bf16[128,512]{1,0:T(8,128)(2,1)S(1)} %constant_dynamic-slice_fusion), channel_id=1, source_target_pairs={{0,6},{2,0},{4,2},{6,4},{1,7},{3,1},{5,3},{7,5},{8,14},{10,8},{12,... | collective-permute-start | bytes 393224 | tf_op jit(solution)/shard_map/ppermute | solution.py:20
  12.9 32.9 %collective-permute-start.12 = (bf16[128,512]{1,0:T(8,128)(2,1)S(1)}, bf16[128,512]{1,0:T(8,128)(2,1)S(1)}, u32[]{:S(2)}, u32[]{:S(2)}) collective-permute-start(bf16[128,512]{1,0:T(8,128)(2,1)S(1)} %constant_dynamic-slice_fusion), channel_id=1, source_target_pairs={{0,2},{2,4},{4,6},{6,0},{1,3},{3,5},{5,7},{7,1},{8,10},{10,12},{12... | collective-permute-start | bytes 393224 | tf_op jit(solution)/shard_map/ppermute | solution.py:20
  25.3 15.5 %copy-start.2 = (bf16[384,128]{1,0:T(8,128)(2,1)}, bf16[384,128]{1,0:T(8,128)(2,1)S(1)}, u32[]{:S(2)}) copy-start(bf16[384,128]{1,0:T(8,128)(2,1)S(1)} %pad_maximum_fusion.3.refs_1_) | copy-start | bytes 294916
  25.3 6.7 %collective-permute-start.8 = (bf16[384,128]{1,0:T(8,128)(2,1)S(1)}, bf16[384,128]{1,0:T(8,128)(2,1)S(1)}, u32[]{:S(2)}, u32[]{:S(2)}) collective-permute-start(bf16[384,128]{1,0:T(8,128)(2,1)S(1)} %pad_maximum_fusion.3.refs_1_), channel_id=1, source_target_pairs={{0,24},{8,16},{16,8},{24,0},{1,25},{9,17},{17,9},{25,1},{2,26},{10... | collective-permute-start | bytes 294920 | tf_op jit(solution)/shard_map/ppermute | solution.py:24
  27.8 10.1 %collective-permute-start.7 = (bf16[384,128]{1,0:T(8,128)(2,1)S(1)}, bf16[384,128]{1,0:T(8,128)(2,1)S(1)}, u32[]{:S(2)}, u32[]{:S(2)}) collective-permute-start(bf16[384,128]{1,0:T(8,128)(2,1)S(1)} %pad_maximum_fusion.3.refs_1_), channel_id=1, source_target_pairs={{0,16},{8,24},{16,0},{24,8},{1,17},{9,25},{17,1},{25,9},{2,18},{10... | collective-permute-start | bytes 294920 | tf_op jit(solution)/shard_map/ppermute | solution.py:24
  28.3 11.2 %collective-permute-start.6 = (bf16[384,128]{1,0:T(8,128)(2,1)S(1)}, bf16[384,128]{1,0:T(8,128)(2,1)S(1)}, u32[]{:S(2)}, u32[]{:S(2)}) collective-permute-start(bf16[384,128]{1,0:T(8,128)(2,1)S(1)} %pad_maximum_fusion.3.refs_1_), channel_id=1, source_target_pairs={{0,8},{8,0},{16,24},{24,16},{1,9},{9,1},{17,25},{25,17},{2,10},{10... | collective-permute-start | bytes 294920 | tf_op jit(solution)/shard_map/ppermute | solution.py:24
  29.0 33.3 %copy-start.3 = (bf16[384,512]{1,0:T(8,128)(2,1)}, bf16[384,512]{1,0:T(8,128)(2,1)S(1)}, u32[]{:S(2)}) copy-start(bf16[384,512]{1,0:T(8,128)(2,1)S(1)} %pad_maximum_fusion.refs_1_) | copy-start | bytes 1179652
  32.0 8.8 %copy-start.7 = (bf16[384,128]{1,0:T(8,128)(2,1)}, bf16[384,128]{1,0:T(8,128)(2,1)S(1)}, u32[]{:S(2)}) copy-start(bf16[384,128]{1,0:T(8,128)(2,1)S(1)} %collective-permute-done.8.refs_4_) | copy-start | bytes 294916
  32.0 28.5 %collective-permute-start.5 = (bf16[384,512]{1,0:T(8,128)(2,1)S(1)}, bf16[384,512]{1,0:T(8,128)(2,1)S(1)}, u32[]{:S(2)}, u32[]{:S(2)}) collective-permute-start(bf16[384,512]{1,0:T(8,128)(2,1)S(1)} %pad_maximum_fusion.refs_1_), channel_id=1, source_target_pairs={{0,24},{8,16},{16,8},{24,0},{1,25},{9,17},{17,9},{25,1},{2,26},{10... | collective-permute-start | bytes 1179656 | tf_op jit(solution)/shard_map/ppermute | solution.py:24
  37.9 2.9 %copy-start.8 = (bf16[384,128]{1,0:T(8,128)(2,1)}, bf16[384,128]{1,0:T(8,128)(2,1)S(1)}, u32[]{:S(2)}) copy-start(bf16[384,128]{1,0:T(8,128)(2,1)S(1)} %collective-permute-done.7.refs_3_) | copy-start | bytes 294916
  37.9 24.3 %collective-permute-start.4 = (bf16[384,512]{1,0:T(8,128)(2,1)S(1)}, bf16[384,512]{1,0:T(8,128)(2,1)S(1)}, u32[]{:S(2)}, u32[]{:S(2)}) collective-permute-start(bf16[384,512]{1,0:T(8,128)(2,1)S(1)} %pad_maximum_fusion.refs_1_), channel_id=1, source_target_pairs={{0,16},{8,24},{16,0},{24,8},{1,17},{9,25},{17,1},{25,9},{2,18},{10... | collective-permute-start | bytes 1179656 | tf_op jit(solution)/shard_map/ppermute | solution.py:24
  39.5 1.3 %copy-start.9 = (bf16[384,128]{1,0:T(8,128)(2,1)}, bf16[384,128]{1,0:T(8,128)(2,1)S(1)}, u32[]{:S(2)}) copy-start(bf16[384,128]{1,0:T(8,128)(2,1)S(1)} %collective-permute-done.6.refs_2_) | copy-start | bytes 294916
  39.5 22.7 %collective-permute-start.3 = (bf16[384,512]{1,0:T(8,128)(2,1)S(1)}, bf16[384,512]{1,0:T(8,128)(2,1)S(1)}, u32[]{:S(2)}, u32[]{:S(2)}) collective-permute-start(bf16[384,512]{1,0:T(8,128)(2,1)S(1)} %pad_maximum_fusion.refs_1_), channel_id=1, source_target_pairs={{0,8},{8,0},{16,24},{24,16},{1,9},{9,1},{17,25},{25,17},{2,10},{10... | collective-permute-start | bytes 1179656 | tf_op jit(solution)/shard_map/ppermute | solution.py:24
  44.0 6.5 %collective-permute-start.13 = (bf16[128,512]{1,0:T(8,128)(2,1)S(1)}, bf16[128,512]{1,0:T(8,128)(2,1)S(1)}, u32[]{:S(2)}, u32[]{:S(2)}) collective-permute-start(bf16[128,512]{1,0:T(8,128)(2,1)S(1)} %constant_dynamic-slice_fusion), channel_id=1, source_target_pairs={{0,4},{2,6},{4,0},{6,2},{1,5},{3,7},{5,1},{7,3},{8,12},{10,14},{12... | collective-permute-start | bytes 393224 | tf_op jit(solution)/shard_map/ppermute | solution.py:20
  45.8 8.9 %collective-permute-start.11 = (bf16[512,128]{1,0:T(8,128)(2,1)}, bf16[512,128]{1,0:T(8,128)(2,1)S(1)}, u32[]{:S(2)}, u32[]{:S(2)}) collective-permute-start(bf16[512,128]{1,0:T(8,128)(2,1)} %shard_map.73.refs_5_), channel_id=1, source_target_pairs={{0,6},{1,7},{8,14},{9,15},{16,22},{17,23},{24,30},{25,31}} | collective-permute-start | bytes 393224 | tf_op jit(solution)/shard_map/ppermute | solution.py:205
  50.5 7.0 %collective-permute-start.10 = (bf16[512,128]{1,0:T(8,128)(2,1)}, bf16[512,128]{1,0:T(8,128)(2,1)S(1)}, u32[]{:S(2)}, u32[]{:S(2)}) collective-permute-start(bf16[512,128]{1,0:T(8,128)(2,1)} %shard_map.73.refs_5_), channel_id=1, source_target_pairs={{0,4},{2,6},{1,5},{3,7},{8,12},{10,14},{9,13},{11,15},{16,20},{18,... | collective-permute-start | bytes 393224 | tf_op jit(solution)/shard_map/ppermute | solution.py:205
  54.7 7.6 %copy-start.13 = (bf16[512,128]{1,0:T(8,128)(2,1)}, bf16[512,128]{1,0:T(8,128)(2,1)S(1)}, u32[]{:S(2)}) copy-start(bf16[512,128]{1,0:T(8,128)(2,1)S(1)} %collective-permute-done.11.refs_8_) | copy-start | bytes 393220
  54.7 5.6 %collective-permute-start.9 = (bf16[512,128]{1,0:T(8,128)(2,1)}, bf16[512,128]{1,0:T(8,128)(2,1)S(1)}, u32[]{:S(2)}, u32[]{:S(2)}) collective-permute-start(bf16[512,128]{1,0:T(8,128)(2,1)} %shard_map.73.refs_5_), channel_id=1, source_target_pairs={{0,2},{2,4},{4,6},{1,3},{3,5},{5,7},{8,10},{10,12},{12,14},{9,11},... | collective-permute-start | bytes 393224 | tf_op jit(solution)/shard_map/ppermute | solution.py:205
  56.1 20.7 %copy-start.1 = (bf16[384,512]{1,0:T(8,128)(2,1)}, bf16[384,512]{1,0:T(8,128)(2,1)S(1)}, u32[]{:S(2)}) copy-start(bf16[384,512]{1,0:T(8,128)(2,1)S(1)} %constant_dynamic-update-slice_fusion.refs_1_) | copy-start | bytes 1179652
  57.5 4.8 %copy-start.14 = (bf16[512,128]{1,0:T(8,128)(2,1)}, bf16[512,128]{1,0:T(8,128)(2,1)S(1)}, u32[]{:S(2)}) copy-start(bf16[512,128]{1,0:T(8,128)(2,1)S(1)} %collective-permute-done.10.refs_7_) | copy-start | bytes 393220
  57.5 19.2 %collective-permute-start.17 = (bf16[384,512]{1,0:T(8,128)(2,1)S(1)}, bf16[384,512]{1,0:T(8,128)(2,1)S(1)}, u32[]{:S(2)}, u32[]{:S(2)}) collective-permute-start(bf16[384,512]{1,0:T(8,128)(2,1)S(1)} %constant_dynamic-update-slice_fusion.refs_1_), channel_id=1, source_target_pairs={{0,24},{8,16},{16,8},{24,0},{1,25},{9,17},{17,9},{25,1},{2,26},{10... | collective-permute-start | bytes 1179656 | tf_op jit(solution)/shard_map/ppermute | solution.py:24
  60.3 2.0 %copy-start.15 = (bf16[512,128]{1,0:T(8,128)(2,1)}, bf16[512,128]{1,0:T(8,128)(2,1)S(1)}, u32[]{:S(2)}) copy-start(bf16[512,128]{1,0:T(8,128)(2,1)S(1)} %collective-permute-done.9.refs_6_) | copy-start | bytes 393220
  60.3 16.4 %collective-permute-start.16 = (bf16[384,512]{1,0:T(8,128)(2,1)S(1)}, bf16[384,512]{1,0:T(8,128)(2,1)S(1)}, u32[]{:S(2)}, u32[]{:S(2)}) collective-permute-start(bf16[384,512]{1,0:T(8,128)(2,1)S(1)} %constant_dynamic-update-slice_fusion.refs_1_), channel_id=1, source_target_pairs={{0,16},{8,24},{16,0},{24,8},{1,17},{9,25},{17,1},{25,9},{2,18},{10... | collective-permute-start | bytes 1179656 | tf_op jit(solution)/shard_map/ppermute | solution.py:24
  60.5 1.8 %copy-start.10 = (bf16[384,512]{1,0:T(8,128)(2,1)}, bf16[384,512]{1,0:T(8,128)(2,1)S(1)}, u32[]{:S(2)}) copy-start(bf16[384,512]{1,0:T(8,128)(2,1)S(1)} %collective-permute-done.5.refs_4_) | copy-start | bytes 1179652
  60.5 16.2 %collective-permute-start.15 = (bf16[384,512]{1,0:T(8,128)(2,1)S(1)}, bf16[384,512]{1,0:T(8,128)(2,1)S(1)}, u32[]{:S(2)}, u32[]{:S(2)}) collective-permute-start(bf16[384,512]{1,0:T(8,128)(2,1)S(1)} %constant_dynamic-update-slice_fusion.refs_1_), channel_id=1, source_target_pairs={{0,8},{8,0},{16,24},{24,16},{1,9},{9,1},{17,25},{25,17},{2,10},{10... | collective-permute-start | bytes 1179656 | tf_op jit(solution)/shard_map/ppermute | solution.py:24
  62.3 0.8 copy-start.11
  63.0 0.7 copy-start.12
  76.7 0.7 copy-start.4
  76.8 0.9 copy-start.5
  77.6 0.7 copy-start.6
  82.4 2.9 %collective-permute-start.18 = (bf16[256,2048]{1,0:T(8,128)(2,1)}, bf16[256,2048]{1,0:T(8,128)(2,1)S(1)}, u32[]{:S(2)}, u32[]{:S(2)}) collective-permute-start(bf16[256,2048]{1,0:T(8,128)(2,1)} %get-tuple-element.8), channel_id=1, source_target_pairs={{0,1},{1,0},{2,3},{3,2},{4,5},{5,4},{6,7},{7,6},{8,9},{9,8},{10,11... | collective-permute-start | bytes 3145736 | tf_op jit(solution)/shard_map/ppermute | solution.py:24
  85.3 1.0 %copy-start = (bf16[256,2048]{1,0:T(8,128)(2,1)}, bf16[256,2048]{1,0:T(8,128)(2,1)S(1)}, u32[]{:S(2)}) copy-start(bf16[256,2048]{1,0:T(8,128)(2,1)S(1)} %collective-permute-done.18.b_ref) | copy-start | bytes 3145732

commit v4 on v3

--- a/solution.py
+++ b/solution.py
@@ -124,7 +124,7 @@
         ).astype(BF16)
         return carry
 
-    lax.fori_loop(0, blocks, one_block, 0, unroll=2)
+    lax.fori_loop(0, blocks, one_block, 0, unroll=4)
 
 
 def project_kernel(where_ref, att_ref, *refs, n_weights, kv_count):
@@ -177,7 +177,8 @@
             axis=1,
         )
         got = along_kv(both, kv_count)
-        pair_shard = jnp.concatenate([key_matrix, value_matrix], axis=1)
+        late_key, late_value, *got = lax.optimization_barrier((key_matrix, value_matrix, *got))
+        pair_shard = jnp.concatenate([late_key, late_value], axis=1)
         pair_parts = across_dp(pair_shard, [g[:, columns:] for g in got], dp_count)
         q_parts = across_dp(query_weight, [g[:, :columns] for g in got], dp_count)
         o_got = along_kv(piece_of(out_weight, dp_count), kv_count)
@@ -244,11 +245,14 @@
         ],
     )(where, attended, *o_parts)
     theirs = swap(other, "tp", 1, tp_count)
+    steps = 4 if out_rows % (4 * ALIGN) == 0 else 1
+    tall = pl.BlockSpec((out_rows // steps, columns), lambda i: (i, 0))
     return pl.pallas_call(
         norm_kernel,
+        grid=(steps,),
         out_shape=jax.ShapeDtypeStruct((out_rows, columns), BF16),
-        in_specs=[vmem, vmem, vmem],
-        out_specs=vmem,
+        in_specs=[tall, tall, pl.BlockSpec((1, columns), lambda i: (0, 0))],
+        out_specs=tall,
     )(mine, theirs, out_gain.reshape(1, -1))
 
 

time: 89.9 us -> 89.2 us (level)
    unnamed x36 -> x40, local copies, waits for them, and re-layouts: 5.97 us -> 4.37 us
  transfers between devices with their start and end apart: 19 -> 19, of which waited for: 6 -> 6; matrix products, arithmetic and copies ran while one was open for 3% -> 3% of each run, Pallas kernels for 18% -> 17%
where the time goes in v4:
time: 89.2 us; the launch traced here: 88.8 us
  starting transfers between devices  31.5 us (35%)
  waiting for transfers between devices  24.9 us (28%)
  Pallas kernels  23.4 us (26%)
  local copies, waits for them, and re-layouts  7.29 us (8%)
  other arithmetic  1.47 us (2%)
    ppermute x6, waiting for transfers between devices, shift(): return lax.ppermute(x, axis, [(i, (i + by) % count) for i in range(count)])  14.2 us
    ppermute x10, starting transfers between devices, swap(): return lax.ppermute(x, axis, [(i, i ^ bit) for i in range(count)])  12.9 us
    pallas_call x1, Pallas kernels, layer(): pl.pallas_call(functools.partial(attend_kernel, n_weights=len(q_parts), n...  12.3 us
    ppermute x6, starting transfers between devices, shift(): return lax.ppermute(x, axis, [(i, (i + by) % count) for i in range(count)])  10.8 us
    ppermute x10, waiting for transfers between devices, swap(): return lax.ppermute(x, axis, [(i, i ^ bit) for i in range(count)])  9.25 us
    ppermute x3, starting transfers between devices, layer(): lax.ppermute(pairs, 'kv', [(i, i + s) for i in range(kv_count - s)])  7.78 us
    unnamed x40, local copies, waits for them, and re-layouts  4.37 us
    pallas_call x1, Pallas kernels, layer(): pl.pallas_call(functools.partial(project_kernel, n_weights=len(o_parts),...  4.04 us
  transfers between devices with their start and end apart: 19, of which 6 were waited for; matrix products, arithmetic and copies ran while one was open for 3% of the time, Pallas kernels for 17%

profile of v4, /device:TPU:0, one launch (start us, length us, event | category | flops | bytes accessed | tf_op | source)
XLA Modules:
  0.0 88.8 jit_solution(6426870653248978105)
XLA Ops:
  0.0 0.8 constant_dynamic-slice_fusion.1
  0.8 0.1 copy.13
  0.9 0.1 copy.12
  1.0 0.9 %constant_dynamic-slice_fusion.3 = bf16[128,512]{1,0:T(8,128)(2,1)S(1)} fusion(bf16[512,512]{1,0:T(8,128)(2,1)} %refs_0_.2, s32[]{:T(128)S(6)} %select_n.2), kind=kLoop, calls=%fused_computation.10 | loop fusion | bytes 262148 | tf_op jit(solution)/shard_map/dynamic_slice | solution.py:29
  2.0 0.1 pad_maximum_fusion.1
  2.1 5.1 %collective-permute-start.2 = (bf16[128,640]{1,0:T(8,128)(2,1)S(1)}, bf16[128,640]{1,0:T(8,128)(2,1)S(1)}, u32[]{:S(2)}, u32[]{:S(2)}) collective-permute-start(bf16[128,640]{1,0:T(8,128)(2,1)S(1)} %pad_maximum_fusion.1), channel_id=1, source_target_pairs={{0,6},{2,0},{4,2},{6,4},{1,7},{3,1},{5,3},{7,5},{8,14},{10,8},{12,... | collective-permute-start | bytes 491528 | tf_op jit(solution)/shard_map/ppermute | solution.py:20
  7.2 0.0 collective-permute-start.1
  7.2 1.0 %collective-permute-start = (bf16[128,640]{1,0:T(8,128)(2,1)S(1)}, bf16[128,640]{1,0:T(8,128)(2,1)S(1)}, u32[]{:S(2)}, u32[]{:S(2)}) collective-permute-start(bf16[128,640]{1,0:T(8,128)(2,1)S(1)} %pad_maximum_fusion.1), channel_id=1, source_target_pairs={{0,2},{2,4},{4,6},{6,0},{1,3},{3,5},{5,7},{7,1},{8,10},{10,12},{12... | collective-permute-start | bytes 491528 | tf_op jit(solution)/shard_map/ppermute | solution.py:20
  8.2 0.9 %constant_dynamic-slice_fusion = bf16[128,512]{1,0:T(8,128)(2,1)S(1)} fusion(bf16[512,512]{1,0:T(8,128)(2,1)} %refs_0_.3, s32[]{:T(128)S(6)} %select_n.2), kind=kLoop, calls=%fused_computation.7 | loop fusion | bytes 262148 | tf_op jit(solution)/shard_map/dynamic_slice | solution.py:29
  9.1 2.9 %collective-permute-start.14 = (bf16[128,512]{1,0:T(8,128)(2,1)S(1)}, bf16[128,512]{1,0:T(8,128)(2,1)S(1)}, u32[]{:S(2)}, u32[]{:S(2)}) collective-permute-start(bf16[128,512]{1,0:T(8,128)(2,1)S(1)} %constant_dynamic-slice_fusion), channel_id=1, source_target_pairs={{0,6},{2,0},{4,2},{6,4},{1,7},{3,1},{5,3},{7,5},{8,14},{10,8},{12,... | collective-permute-start | bytes 393224 | tf_op jit(solution)/shard_map/ppermute | solution.py:20
  12.0 0.0 collective-permute-start.12
  12.0 0.6 pad_add_fusion.where_ref
  12.6 0.0 collective-permute-done.2
  12.6 11.8 %collective-permute-done.1 = bf16[128,640]{1,0:T(8,128)(2,1)S(1)} collective-permute-done((bf16[128,640]{1,0:T(8,128)(2,1)S(1)}, bf16[128,640]{1,0:T(8,128)(2,1)S(1)}, u32[]{:S(2)}, u32[]{:S(2)}) %collective-permute-start.1) | collective-permute-done | bytes 163872 | tf_op jit(solution)/shard_map/ppermute | solution.py:20
  24.4 0.0 collective-permute-done
  24.5 0.0 copy-start.2
  24.5 2.5 %collective-permute-start.8 = (bf16[384,128]{1,0:T(8,128)(2,1)S(1)}, bf16[384,128]{1,0:T(8,128)(2,1)S(1)}, u32[]{:S(2)}, u32[]{:S(2)}) collective-permute-start(bf16[384,128]{1,0:T(8,128)(2,1)S(1)} %pad_maximum_fusion.3.refs_1_), channel_id=1, source_target_pairs={{0,24},{8,16},{16,8},{24,0},{1,25},{9,17},{17,9},{25,1},{2,26},{10... | collective-permute-start | bytes 294920 | tf_op jit(solution)/shard_map/ppermute | solution.py:24
  27.0 0.5 collective-permute-start.7
  27.5 0.5 collective-permute-start.6
  28.1 0.0 copy-done.7
  28.1 0.0 copy-start.3
  28.1 0.1 copy.10
  28.2 0.0 copy-done.8
  28.2 0.1 copy.11
  28.3 2.8 %collective-permute-done.8.refs_4_ = bf16[384,128]{1,0:T(8,128)(2,1)S(1)} collective-permute-done((bf16[384,128]{1,0:T(8,128)(2,1)S(1)}, bf16[384,128]{1,0:T(8,128)(2,1)S(1)}, u32[]{:S(2)}, u32[]{:S(2)}) %collective-permute-start.8) | collective-permute-done | bytes 98336 | tf_op jit(solution)/shard_map/ppermute | solution.py:24
  31.2 2.4 %collective-permute-start.5 = (bf16[384,512]{1,0:T(8,128)(2,1)S(1)}, bf16[384,512]{1,0:T(8,128)(2,1)S(1)}, u32[]{:S(2)}, u32[]{:S(2)}) collective-permute-start(bf16[384,512]{1,0:T(8,128)(2,1)S(1)} %pad_maximum_fusion.refs_1_), channel_id=1, source_target_pairs={{0,24},{8,16},{16,8},{24,0},{1,25},{9,17},{17,9},{25,1},{2,26},{10... | collective-permute-start | bytes 1179656 | tf_op jit(solution)/shard_map/ppermute | solution.py:24
  33.6 3.5 %collective-permute-done.7.refs_3_ = bf16[384,128]{1,0:T(8,128)(2,1)S(1)} collective-permute-done((bf16[384,128]{1,0:T(8,128)(2,1)S(1)}, bf16[384,128]{1,0:T(8,128)(2,1)S(1)}, u32[]{:S(2)}, u32[]{:S(2)}) %collective-permute-start.7) | collective-permute-done | bytes 98336 | tf_op jit(solution)/shard_map/ppermute | solution.py:24
  37.1 1.6 %collective-permute-start.4 = (bf16[384,512]{1,0:T(8,128)(2,1)S(1)}, bf16[384,512]{1,0:T(8,128)(2,1)S(1)}, u32[]{:S(2)}, u32[]{:S(2)}) collective-permute-start(bf16[384,512]{1,0:T(8,128)(2,1)S(1)} %pad_maximum_fusion.refs_1_), channel_id=1, source_target_pairs={{0,16},{8,24},{16,0},{24,8},{1,17},{9,25},{17,1},{25,9},{2,18},{10... | collective-permute-start | bytes 1179656 | tf_op jit(solution)/shard_map/ppermute | solution.py:24
  38.7 0.0 collective-permute-done.6.refs_2_
  38.7 0.6 collective-permute-start.3
  39.3 0.8 pad_maximum_fusion.2.refs_0_
  40.1 3.2 %shard_map.73.refs_5_ = bf16[512,128]{1,0:T(8,128)(2,1)} custom-call(s32[3]{0:T(128)} %pad_add_fusion.where_ref, bf16[512,2048]{1,0:T(8,128)(2,1)} %tok_ref.3, bf16[512,128]{1,0:T(8,128)(2,1)} %pad_maximum_fusion.2.refs_0_, bf16[384,128]{1,0:T(8,128)(2,1)} %copy-done.2, bf16[384,128]{1,0:T(8,128)(2,1)} %copy-done.11, bf16[384,128]{1,0:T(8,128)(2,1)} %copy-done.10, ...), custom_call_target="tpu_custom_call" | custom-call | tf_op jit(solution)/shard_map/pallas_call | solution.py:194
  43.3 0.0 collective-permute-done.14
  43.3 1.8 %collective-permute-start.13 = (bf16[128,512]{1,0:T(8,128)(2,1)S(1)}, bf16[128,512]{1,0:T(8,128)(2,1)S(1)}, u32[]{:S(2)}, u32[]{:S(2)}) collective-permute-start(bf16[128,512]{1,0:T(8,128)(2,1)S(1)} %constant_dynamic-slice_fusion), channel_id=1, source_target_pairs={{0,4},{2,6},{4,0},{6,2},{1,5},{3,7},{5,1},{7,3},{8,12},{10,14},{12... | collective-permute-start | bytes 393224 | tf_op jit(solution)/shard_map/ppermute | solution.py:20
  45.0 0.0 collective-permute-done.12
  45.0 2.3 %collective-permute-start.11 = (bf16[512,128]{1,0:T(8,128)(2,1)}, bf16[512,128]{1,0:T(8,128)(2,1)S(1)}, u32[]{:S(2)}, u32[]{:S(2)}) collective-permute-start(bf16[512,128]{1,0:T(8,128)(2,1)} %shard_map.73.refs_5_), channel_id=1, source_target_pairs={{0,6},{1,7},{8,14},{9,15},{16,22},{17,23},{24,30},{25,31}} | collective-permute-start | bytes 393224 | tf_op jit(solution)/shard_map/ppermute | solution.py:206
  47.4 2.4 %collective-permute-done.13 = bf16[128,512]{1,0:T(8,128)(2,1)S(1)} collective-permute-done((bf16[128,512]{1,0:T(8,128)(2,1)S(1)}, bf16[128,512]{1,0:T(8,128)(2,1)S(1)}, u32[]{:S(2)}, u32[]{:S(2)}) %collective-permute-start.13) | collective-permute-done | bytes 131104 | tf_op jit(solution)/shard_map/ppermute | solution.py:20
  49.8 4.1 %collective-permute-start.10 = (bf16[512,128]{1,0:T(8,128)(2,1)}, bf16[512,128]{1,0:T(8,128)(2,1)S(1)}, u32[]{:S(2)}, u32[]{:S(2)}) collective-permute-start(bf16[512,128]{1,0:T(8,128)(2,1)} %shard_map.73.refs_5_), channel_id=1, source_target_pairs={{0,4},{2,6},{1,5},{3,7},{8,12},{10,14},{9,13},{11,15},{16,20},{18,... | collective-permute-start | bytes 393224 | tf_op jit(solution)/shard_map/ppermute | solution.py:206
  54.0 0.0 collective-permute-done.11.refs_8_
  54.0 0.0 copy-start.15
  54.0 1.3 %collective-permute-start.9 = (bf16[512,128]{1,0:T(8,128)(2,1)}, bf16[512,128]{1,0:T(8,128)(2,1)S(1)}, u32[]{:S(2)}, u32[]{:S(2)}) collective-permute-start(bf16[512,128]{1,0:T(8,128)(2,1)} %shard_map.73.refs_5_), channel_id=1, source_target_pairs={{0,2},{2,4},{4,6},{1,3},{3,5},{5,7},{8,10},{10,12},{12,14},{9,11},... | collective-permute-start | bytes 393224 | tf_op jit(solution)/shard_map/ppermute | solution.py:206
  55.3 1.4 %collective-permute-done.10.refs_7_ = bf16[512,128]{1,0:T(8,128)(2,1)S(1)} collective-permute-done((bf16[512,128]{1,0:T(8,128)(2,1)}, bf16[512,128]{1,0:T(8,128)(2,1)S(1)}, u32[]{:S(2)}, u32[]{:S(2)}) %collective-permute-start.10) | collective-permute-done | bytes 131104 | tf_op jit(solution)/shard_map/ppermute | solution.py:206
  56.8 2.8 %collective-permute-start.17 = (bf16[384,512]{1,0:T(8,128)(2,1)S(1)}, bf16[384,512]{1,0:T(8,128)(2,1)S(1)}, u32[]{:S(2)}, u32[]{:S(2)}) collective-permute-start(bf16[384,512]{1,0:T(8,128)(2,1)S(1)} %constant_dynamic-update-slice_fusion.refs_1_), channel_id=1, source_target_pairs={{0,24},{8,16},{16,8},{24,0},{1,25},{9,17},{17,9},{25,1},{2,26},{10... | collective-permute-start | bytes 1179656 | tf_op jit(solution)/shard_map/ppermute | solution.py:24
  59.6 0.0 collective-permute-done.9.refs_6_
  59.6 0.2 collective-permute-start.16
  59.8 0.0 collective-permute-done.5.refs_4_
  59.8 1.7 %collective-permute-start.15 = (bf16[384,512]{1,0:T(8,128)(2,1)S(1)}, bf16[384,512]{1,0:T(8,128)(2,1)S(1)}, u32[]{:S(2)}, u32[]{:S(2)}) collective-permute-start(bf16[384,512]{1,0:T(8,128)(2,1)S(1)} %constant_dynamic-update-slice_fusion.refs_1_), channel_id=1, source_target_pairs={{0,8},{8,0},{16,24},{24,16},{1,9},{9,1},{17,25},{25,17},{2,10},{10... | collective-permute-start | bytes 1179656 | tf_op jit(solution)/shard_map/ppermute | solution.py:24
  61.5 0.0 collective-permute-done.4.refs_3_
  61.5 0.0 collective-permute-done.3.refs_2_
  61.6 0.7 copy-done.13
  62.3 0.8 copy-done.14
  63.1 12.3 %shard_map.74.att_ref = bf16[512,512]{1,0:T(8,128)(2,1)} custom-call(s32[3]{0:T(128)} %pad_add_fusion.where_ref, s32[8,16]{1,0:T(8,128)} %chosen_ref.1, bf16[512,2048]{1,0:T(8,128)(2,1)} %tok_ref.3, bf16[512,512]{1,0:T(8,128)(2,1)} %refs_0_.2, bf16[384,512]{1,0:T(8,128)(2,1)} %copy-done.3, bf16[384,512]{1,0:T(8,128)(2,1)} %copy-done.14, ...), custom_call_target="tpu_custom_call" | custom-call | flops 34359738368 | bytes 2097152 | tf_op jit(solution)/shard_map/pallas_call | solution.py:209
  75.4 0.0 collective-permute-done.17.refs_4_
  75.4 0.0 collective-permute-done.16.refs_3_
  75.4 0.0 copy-start.5
  75.4 0.0 collective-permute-done.15.refs_2_
  75.4 0.7 copy-done.4
  76.1 0.2 copy-done.5
  76.3 0.7 copy-done.6
  77.0 4.0 %shard_map.75 = (bf16[256,2048]{1,0:T(8,128)(2,1)}, bf16[256,2048]{1,0:T(8,128)(2,1)}) custom-call(s32[3]{0:T(128)} %pad_add_fusion.where_ref, bf16[512,512]{1,0:T(8,128)(2,1)} %shard_map.74.att_ref, bf16[512,512]{1,0:T(8,128)(2,1)} %refs_0_.3, bf16[384,512]{1,0:T(8,128)(2,1)} %copy-done.1, bf16[384,512]{1,0:T(8,128)(2,1)} %copy-done.6, ...), custom_call_target="tpu_custom_call" | custom-call | tf_op jit(solution)/shard_map/pallas_call | solution.py:236
  81.1 0.0 collective-permute-start.18
  81.1 2.9 %collective-permute-done.18.b_ref = bf16[256,2048]{1,0:T(8,128)(2,1)S(1)} collective-permute-done((bf16[256,2048]{1,0:T(8,128)(2,1)}, bf16[256,2048]{1,0:T(8,128)(2,1)S(1)}, u32[]{:S(2)}, u32[]{:S(2)}) %collective-permute-start.18) | collective-permute-done | bytes 1048608 | tf_op jit(solution)/shard_map/ppermute | solution.py:24
  83.9 1.0 %copy-done = bf16[256,2048]{1,0:T(8,128)(2,1)} copy-done((bf16[256,2048]{1,0:T(8,128)(2,1)}, bf16[256,2048]{1,0:T(8,128)(2,1)S(1)}, u32[]{:S(2)}) %copy-start) | copy-done | bytes 1048600
  84.9 3.9 %shard_map.76 = bf16[256,2048]{1,0:T(8,128)(2,1)} custom-call(bf16[256,2048]{1,0:T(8,128)(2,1)} %get-tuple-element.17.a_ref, bf16[256,2048]{1,0:T(8,128)(2,1)} %copy-done, f32[1,2048]{1,0:T(1,128)} %bitcast.4), custom_call_target="tpu_custom_call" | custom-call | tf_op jit(solution)/shard_map/pallas_call | solution.py:250
  (35 shorter events, 0.2 us)
Async XLA Ops:
  0.0 28.2 %copy-start.8 = (bf16[512,64]{0,1:T(8,128)(2,1)S(1)}, bf16[512,64]{0,1:T(8,128)(2,1)}, u32[]{:S(2)}) copy-start(bf16[512,64]{0,1:T(8,128)(2,1)} %param.11) | copy-start | bytes 196612
  0.0 28.1 %copy-start.7 = (bf16[512,64]{0,1:T(8,128)(2,1)S(1)}, bf16[512,64]{0,1:T(8,128)(2,1)}, u32[]{:S(2)}) copy-start(bf16[512,64]{0,1:T(8,128)(2,1)} %param.10) | copy-start | bytes 196612
  2.1 10.5 %collective-permute-start.2 = (bf16[128,640]{1,0:T(8,128)(2,1)S(1)}, bf16[128,640]{1,0:T(8,128)(2,1)S(1)}, u32[]{:S(2)}, u32[]{:S(2)}) collective-permute-start(bf16[128,640]{1,0:T(8,128)(2,1)S(1)} %pad_maximum_fusion.1), channel_id=1, source_target_pairs={{0,6},{2,0},{4,2},{6,4},{1,7},{3,1},{5,3},{7,5},{8,14},{10,8},{12,... | collective-permute-start | bytes 491528 | tf_op jit(solution)/shard_map/ppermute | solution.py:20
  7.2 17.2 %collective-permute-start.1 = (bf16[128,640]{1,0:T(8,128)(2,1)S(1)}, bf16[128,640]{1,0:T(8,128)(2,1)S(1)}, u32[]{:S(2)}, u32[]{:S(2)}) collective-permute-start(bf16[128,640]{1,0:T(8,128)(2,1)S(1)} %pad_maximum_fusion.1), channel_id=1, source_target_pairs={{0,4},{2,6},{4,0},{6,2},{1,5},{3,7},{5,1},{7,3},{8,12},{10,14},{12... | collective-permute-start | bytes 491528 | tf_op jit(solution)/shard_map/ppermute | solution.py:20
  7.2 17.2 %collective-permute-start = (bf16[128,640]{1,0:T(8,128)(2,1)S(1)}, bf16[128,640]{1,0:T(8,128)(2,1)S(1)}, u32[]{:S(2)}, u32[]{:S(2)}) collective-permute-start(bf16[128,640]{1,0:T(8,128)(2,1)S(1)} %pad_maximum_fusion.1), channel_id=1, source_target_pairs={{0,2},{2,4},{4,6},{6,0},{1,3},{3,5},{5,7},{7,1},{8,10},{10,12},{12... | collective-permute-start | bytes 491528 | tf_op jit(solution)/shard_map/ppermute | solution.py:20
  9.1 34.2 %collective-permute-start.14 = (bf16[128,512]{1,0:T(8,128)(2,1)S(1)}, bf16[128,512]{1,0:T(8,128)(2,1)S(1)}, u32[]{:S(2)}, u32[]{:S(2)}) collective-permute-start(bf16[128,512]{1,0:T(8,128)(2,1)S(1)} %constant_dynamic-slice_fusion), channel_id=1, source_target_pairs={{0,6},{2,0},{4,2},{6,4},{1,7},{3,1},{5,3},{7,5},{8,14},{10,8},{12,... | collective-permute-start | bytes 393224 | tf_op jit(solution)/shard_map/ppermute | solution.py:20
  12.0 33.0 %collective-permute-start.12 = (bf16[128,512]{1,0:T(8,128)(2,1)S(1)}, bf16[128,512]{1,0:T(8,128)(2,1)S(1)}, u32[]{:S(2)}, u32[]{:S(2)}) collective-permute-start(bf16[128,512]{1,0:T(8,128)(2,1)S(1)} %constant_dynamic-slice_fusion), channel_id=1, source_target_pairs={{0,2},{2,4},{4,6},{6,0},{1,3},{3,5},{5,7},{7,1},{8,10},{10,12},{12... | collective-permute-start | bytes 393224 | tf_op jit(solution)/shard_map/ppermute | solution.py:20
  24.5 15.6 %copy-start.2 = (bf16[384,128]{1,0:T(8,128)(2,1)}, bf16[384,128]{1,0:T(8,128)(2,1)S(1)}, u32[]{:S(2)}) copy-start(bf16[384,128]{1,0:T(8,128)(2,1)S(1)} %pad_maximum_fusion.3.refs_1_) | copy-start | bytes 294916
  24.5 6.7 %collective-permute-start.8 = (bf16[384,128]{1,0:T(8,128)(2,1)S(1)}, bf16[384,128]{1,0:T(8,128)(2,1)S(1)}, u32[]{:S(2)}, u32[]{:S(2)}) collective-permute-start(bf16[384,128]{1,0:T(8,128)(2,1)S(1)} %pad_maximum_fusion.3.refs_1_), channel_id=1, source_target_pairs={{0,24},{8,16},{16,8},{24,0},{1,25},{9,17},{17,9},{25,1},{2,26},{10... | collective-permute-start | bytes 294920 | tf_op jit(solution)/shard_map/ppermute | solution.py:24
  27.0 10.1 %collective-permute-start.7 = (bf16[384,128]{1,0:T(8,128)(2,1)S(1)}, bf16[384,128]{1,0:T(8,128)(2,1)S(1)}, u32[]{:S(2)}, u32[]{:S(2)}) collective-permute-start(bf16[384,128]{1,0:T(8,128)(2,1)S(1)} %pad_maximum_fusion.3.refs_1_), channel_id=1, source_target_pairs={{0,16},{8,24},{16,0},{24,8},{1,17},{9,25},{17,1},{25,9},{2,18},{10... | collective-permute-start | bytes 294920 | tf_op jit(solution)/shard_map/ppermute | solution.py:24
  27.5 11.2 %collective-permute-start.6 = (bf16[384,128]{1,0:T(8,128)(2,1)S(1)}, bf16[384,128]{1,0:T(8,128)(2,1)S(1)}, u32[]{:S(2)}, u32[]{:S(2)}) collective-permute-start(bf16[384,128]{1,0:T(8,128)(2,1)S(1)} %pad_maximum_fusion.3.refs_1_), channel_id=1, source_target_pairs={{0,8},{8,0},{16,24},{24,16},{1,9},{9,1},{17,25},{25,17},{2,10},{10... | collective-permute-start | bytes 294920 | tf_op jit(solution)/shard_map/ppermute | solution.py:24
  28.1 27.3 %copy-start.3 = (bf16[384,512]{1,0:T(8,128)(2,1)}, bf16[384,512]{1,0:T(8,128)(2,1)S(1)}, u32[]{:S(2)}) copy-start(bf16[384,512]{1,0:T(8,128)(2,1)S(1)} %pad_maximum_fusion.refs_1_) | copy-start | bytes 1179652
  31.2 8.9 %copy-start.9 = (bf16[384,128]{1,0:T(8,128)(2,1)}, bf16[384,128]{1,0:T(8,128)(2,1)S(1)}, u32[]{:S(2)}) copy-start(bf16[384,128]{1,0:T(8,128)(2,1)S(1)} %collective-permute-done.8.refs_4_) | copy-start | bytes 294916
  31.2 28.6 %collective-permute-start.5 = (bf16[384,512]{1,0:T(8,128)(2,1)S(1)}, bf16[384,512]{1,0:T(8,128)(2,1)S(1)}, u32[]{:S(2)}, u32[]{:S(2)}) collective-permute-start(bf16[384,512]{1,0:T(8,128)(2,1)S(1)} %pad_maximum_fusion.refs_1_), channel_id=1, source_target_pairs={{0,24},{8,16},{16,8},{24,0},{1,25},{9,17},{17,9},{25,1},{2,26},{10... | collective-permute-start | bytes 1179656 | tf_op jit(solution)/shard_map/ppermute | solution.py:24
  37.1 3.0 %copy-start.10 = (bf16[384,128]{1,0:T(8,128)(2,1)}, bf16[384,128]{1,0:T(8,128)(2,1)S(1)}, u32[]{:S(2)}) copy-start(bf16[384,128]{1,0:T(8,128)(2,1)S(1)} %collective-permute-done.7.refs_3_) | copy-start | bytes 294916
  37.1 24.4 %collective-permute-start.4 = (bf16[384,512]{1,0:T(8,128)(2,1)S(1)}, bf16[384,512]{1,0:T(8,128)(2,1)S(1)}, u32[]{:S(2)}, u32[]{:S(2)}) collective-permute-start(bf16[384,512]{1,0:T(8,128)(2,1)S(1)} %pad_maximum_fusion.refs_1_), channel_id=1, source_target_pairs={{0,16},{8,24},{16,0},{24,8},{1,17},{9,25},{17,1},{25,9},{2,18},{10... | collective-permute-start | bytes 1179656 | tf_op jit(solution)/shard_map/ppermute | solution.py:24
  38.7 1.4 %copy-start.11 = (bf16[384,128]{1,0:T(8,128)(2,1)}, bf16[384,128]{1,0:T(8,128)(2,1)S(1)}, u32[]{:S(2)}) copy-start(bf16[384,128]{1,0:T(8,128)(2,1)S(1)} %collective-permute-done.6.refs_2_) | copy-start | bytes 294916
  38.7 22.8 %collective-permute-start.3 = (bf16[384,512]{1,0:T(8,128)(2,1)S(1)}, bf16[384,512]{1,0:T(8,128)(2,1)S(1)}, u32[]{:S(2)}, u32[]{:S(2)}) collective-permute-start(bf16[384,512]{1,0:T(8,128)(2,1)S(1)} %pad_maximum_fusion.refs_1_), channel_id=1, source_target_pairs={{0,8},{8,0},{16,24},{24,16},{1,9},{9,1},{17,25},{25,17},{2,10},{10... | collective-permute-start | bytes 1179656 | tf_op jit(solution)/shard_map/ppermute | solution.py:24
  43.3 6.5 %collective-permute-start.13 = (bf16[128,512]{1,0:T(8,128)(2,1)S(1)}, bf16[128,512]{1,0:T(8,128)(2,1)S(1)}, u32[]{:S(2)}, u32[]{:S(2)}) collective-permute-start(bf16[128,512]{1,0:T(8,128)(2,1)S(1)} %constant_dynamic-slice_fusion), channel_id=1, source_target_pairs={{0,4},{2,6},{4,0},{6,2},{1,5},{3,7},{5,1},{7,3},{8,12},{10,14},{12... | collective-permute-start | bytes 393224 | tf_op jit(solution)/shard_map/ppermute | solution.py:20
  45.0 8.9 %collective-permute-start.11 = (bf16[512,128]{1,0:T(8,128)(2,1)}, bf16[512,128]{1,0:T(8,128)(2,1)S(1)}, u32[]{:S(2)}, u32[]{:S(2)}) collective-permute-start(bf16[512,128]{1,0:T(8,128)(2,1)} %shard_map.73.refs_5_), channel_id=1, source_target_pairs={{0,6},{1,7},{8,14},{9,15},{16,22},{17,23},{24,30},{25,31}} | collective-permute-start | bytes 393224 | tf_op jit(solution)/shard_map/ppermute | solution.py:206
  49.8 7.0 %collective-permute-start.10 = (bf16[512,128]{1,0:T(8,128)(2,1)}, bf16[512,128]{1,0:T(8,128)(2,1)S(1)}, u32[]{:S(2)}, u32[]{:S(2)}) collective-permute-start(bf16[512,128]{1,0:T(8,128)(2,1)} %shard_map.73.refs_5_), channel_id=1, source_target_pairs={{0,4},{2,6},{1,5},{3,7},{8,12},{10,14},{9,13},{11,15},{16,20},{18,... | collective-permute-start | bytes 393224 | tf_op jit(solution)/shard_map/ppermute | solution.py:206
  54.0 7.6 %copy-start.15 = (bf16[512,128]{1,0:T(8,128)(2,1)}, bf16[512,128]{1,0:T(8,128)(2,1)S(1)}, u32[]{:S(2)}) copy-start(bf16[512,128]{1,0:T(8,128)(2,1)S(1)} %collective-permute-done.11.refs_8_) | copy-start | bytes 393220
  54.0 5.6 %collective-permute-start.9 = (bf16[512,128]{1,0:T(8,128)(2,1)}, bf16[512,128]{1,0:T(8,128)(2,1)S(1)}, u32[]{:S(2)}, u32[]{:S(2)}) collective-permute-start(bf16[512,128]{1,0:T(8,128)(2,1)} %shard_map.73.refs_5_), channel_id=1, source_target_pairs={{0,2},{2,4},{4,6},{1,3},{3,5},{5,7},{8,10},{10,12},{12,14},{9,11},... | collective-permute-start | bytes 393224 | tf_op jit(solution)/shard_map/ppermute | solution.py:206
  55.3 20.0 %copy-start.1 = (bf16[384,512]{1,0:T(8,128)(2,1)}, bf16[384,512]{1,0:T(8,128)(2,1)S(1)}, u32[]{:S(2)}) copy-start(bf16[384,512]{1,0:T(8,128)(2,1)S(1)} %constant_dynamic-update-slice_fusion.refs_1_) | copy-start | bytes 1179652
  56.8 4.8 %copy-start.16 = (bf16[512,128]{1,0:T(8,128)(2,1)}, bf16[512,128]{1,0:T(8,128)(2,1)S(1)}, u32[]{:S(2)}) copy-start(bf16[512,128]{1,0:T(8,128)(2,1)S(1)} %collective-permute-done.10.refs_7_) | copy-start | bytes 393220
  56.8 18.6 %collective-permute-start.17 = (bf16[384,512]{1,0:T(8,128)(2,1)S(1)}, bf16[384,512]{1,0:T(8,128)(2,1)S(1)}, u32[]{:S(2)}, u32[]{:S(2)}) collective-permute-start(bf16[384,512]{1,0:T(8,128)(2,1)S(1)} %constant_dynamic-update-slice_fusion.refs_1_), channel_id=1, source_target_pairs={{0,24},{8,16},{16,8},{24,0},{1,25},{9,17},{17,9},{25,1},{2,26},{10... | collective-permute-start | bytes 1179656 | tf_op jit(solution)/shard_map/ppermute | solution.py:24
  59.6 2.0 %copy-start.17 = (bf16[512,128]{1,0:T(8,128)(2,1)}, bf16[512,128]{1,0:T(8,128)(2,1)S(1)}, u32[]{:S(2)}) copy-start(bf16[512,128]{1,0:T(8,128)(2,1)S(1)} %collective-permute-done.9.refs_6_) | copy-start | bytes 393220
  59.6 15.8 %collective-permute-start.16 = (bf16[384,512]{1,0:T(8,128)(2,1)S(1)}, bf16[384,512]{1,0:T(8,128)(2,1)S(1)}, u32[]{:S(2)}, u32[]{:S(2)}) collective-permute-start(bf16[384,512]{1,0:T(8,128)(2,1)S(1)} %constant_dynamic-update-slice_fusion.refs_1_), channel_id=1, source_target_pairs={{0,16},{8,24},{16,0},{24,8},{1,17},{9,25},{17,1},{25,9},{2,18},{10... | collective-permute-start | bytes 1179656 | tf_op jit(solution)/shard_map/ppermute | solution.py:24
  59.8 1.8 %copy-start.12 = (bf16[384,512]{1,0:T(8,128)(2,1)}, bf16[384,512]{1,0:T(8,128)(2,1)S(1)}, u32[]{:S(2)}) copy-start(bf16[384,512]{1,0:T(8,128)(2,1)S(1)} %collective-permute-done.5.refs_4_) | copy-start | bytes 1179652
  59.8 15.6 %collective-permute-start.15 = (bf16[384,512]{1,0:T(8,128)(2,1)S(1)}, bf16[384,512]{1,0:T(8,128)(2,1)S(1)}, u32[]{:S(2)}, u32[]{:S(2)}) collective-permute-start(bf16[384,512]{1,0:T(8,128)(2,1)S(1)} %constant_dynamic-update-slice_fusion.refs_1_), channel_id=1, source_target_pairs={{0,8},{8,0},{16,24},{24,16},{1,9},{9,1},{17,25},{25,17},{2,10},{10... | collective-permute-start | bytes 1179656 | tf_op jit(solution)/shard_map/ppermute | solution.py:24
  61.5 0.8 copy-start.13
  62.3 0.8 copy-start.14
  75.4 0.8 copy-start.4
  75.4 0.9 %copy-start.5 = (bf16[384,512]{1,0:T(8,128)(2,1)}, bf16[384,512]{1,0:T(8,128)(2,1)S(1)}, u32[]{:S(2)}) copy-start(bf16[384,512]{1,0:T(8,128)(2,1)S(1)} %collective-permute-done.16.refs_3_) | copy-start | bytes 1179652
  76.3 0.7 copy-start.6
  81.1 2.9 %collective-permute-start.18 = (bf16[256,2048]{1,0:T(8,128)(2,1)}, bf16[256,2048]{1,0:T(8,128)(2,1)S(1)}, u32[]{:S(2)}, u32[]{:S(2)}) collective-permute-start(bf16[256,2048]{1,0:T(8,128)(2,1)} %get-tuple-element.18), channel_id=1, source_target_pairs={{0,1},{1,0},{2,3},{3,2},{4,5},{5,4},{6,7},{7,6},{8,9},{9,8},{10,11... | collective-permute-start | bytes 3145736 | tf_op jit(solution)/shard_map/ppermute | solution.py:24
  83.9 1.0 %copy-start = (bf16[256,2048]{1,0:T(8,128)(2,1)}, bf16[256,2048]{1,0:T(8,128)(2,1)S(1)}, u32[]{:S(2)}) copy-start(bf16[256,2048]{1,0:T(8,128)(2,1)S(1)} %collective-permute-done.18.b_ref) | copy-start | bytes 3145732
